TPU v7x, 32 devices: a whole 2x2x4 slice. The times are simulated.
32 devices in a mesh: rep: 2 (over x), fs: 4 (over z), tp: 4 (over y, core).
Axes of the slice: x: 2, y: 2, z: 4, core: 2. Of those that a mesh axis runs over, the one named last changes fastest.
Arguments:
- tokens: bfloat16 [4096, 2048], P(('rep', 'fs', 'tp')), may hold values from -6 to 6
- mix_gain: bfloat16 [2048], replicated, may hold values from 0.099609375 to 1.8984375
- gate_proj: bfloat16 [2048, 512], P('fs', 'tp'), may hold values from -0.125 to 0.125
- value_proj: bfloat16 [2048, 512], P('fs', 'tp'), may hold values from -1 to 1
- layer_gain: bfloat16 [512], replicated, may hold values from 0.099609375 to 1.8984375
- layer_shift: bfloat16 [512], replicated, may hold values from -3 to 3
- mix_kernel: bfloat16 [4, 128, 128], replicated, may hold values from -0.5 to 0.5
- mix_offset: bfloat16 [4, 128], replicated, may hold values from -4 to 4
- out_proj: bfloat16 [2048, 512], P('fs', 'tp'), may hold values from -0.25 to 0.25
- ffn_gain: bfloat16 [2048], replicated, may hold values from 0.099609375 to 1.8984375
- ffn_gate: bfloat16 [2048, 5632], P('fs', 'tp'), may hold values from -0.125 to 0.125
- ffn_up: bfloat16 [2048, 5632], P('fs', 'tp'), may hold values from -0.125 to 0.125
- ffn_down: bfloat16 [2048, 5632], P('fs', 'tp'), may hold values from -0.078125 to 0.078125
Outputs:
- layer_out: bfloat16 [4096, 2048], P(('rep', 'fs', 'tp'))
All inputs are finite; a program needn't handle non-finite values.
Results may differ from a plain program's by a relative error of at most 0.015.
Values may be sent and summed in bfloat16 or wider, within the bound.
No kernel may reach another device: no remote copies, remote signals or barrier semaphores. Data moves between devices by JAX's collectives and lax.ppermute only.
A program may use at most 64 MiB of HBM per device.

v0:
```python
import functools

import jax
import jax.numpy as jnp
from jax import lax
from jax.experimental import pallas as pl
from jax.experimental.pallas import tpu as pltpu
from jax.sharding import PartitionSpec as P


epsilon = 1e-06
f32, bf16 = jnp.float32, jnp.bfloat16
MIB = 1024 * 1024


def xor_permute(x, axis, m, n):
    return lax.ppermute(x, axis, [(i, i ^ m) for i in range(n)])


def bits(n, low=1):
    out = []
    while low < n:
        out.append(low)
        low *= 2
    return out


def absolute(items, me):
    items = list(items)
    for m in bits(len(items)):
        flip = (me & m) != 0
        items = [jnp.where(flip, items[i ^ m], items[i]) for i in range(len(items))]
    return items


def contract_last(left, right):
    return lax.dot_general(left, right, (((1,), (1,)), ((), ())), preferred_element_type=f32)


def pack_kernel(part, *refs):
    weights, (full, mine, sem) = refs[:-3], refs[-3:]
    base = pl.multiple_of(lax.axis_index("rep") * part, part)
    copies = []
    for i, ref in enumerate(weights):
        copies.append(
            pltpu.make_async_copy(ref.at[pl.ds(base, part)], mine.at[i], sem.at[len(copies)])
        )
        copies.append(pltpu.make_async_copy(ref, full.at[i], sem.at[len(copies)]))
    for c in copies:
        c.start()
    for c in copies:
        c.wait()


def mixer_kernel(cfg, tok, gain, lgain, lshift, mkern, moff, fgain, *rest):
    bundles, (mid, normed2, wbuf, sem) = rest[: len(cfg["segments"])], rest[len(cfg["segments"]) :]
    k, r, t = lax.axis_index("fs"), lax.axis_index("rep"), lax.axis_index("tp")
    rows, part, lw, width = cfg["rows"], cfg["part"], cfg["lw"], cfg["width"]
    copies = []
    for ref, segs in zip(bundles, cfg["segments"]):
        for start, count, j, rr, tt in segs:
            base = (k ^ j) * rows
            if rr is not None:
                base = base + (r ^ rr) * part
            copies.append(
                pltpu.make_async_copy(
                    ref.at[:, pl.ds(start, count)],
                    wbuf.at[tt, :, pl.ds(pl.multiple_of(base, part), count)],
                    sem.at[len(copies)],
                )
            )
    for c in copies:
        c.start()
    x = tok[...].astype(f32)
    scale = lax.rsqrt(jnp.mean(x * x, axis=-1, keepdims=True) + epsilon)
    normed = (x * scale * gain[...].astype(f32)).astype(bf16)
    for c in copies:
        c.wait()
    n_tp = wbuf.shape[0]
    gate_u, act = [], []
    total = squares = 0.0
    for tt in range(n_tp):
        gate_u.append(jax.nn.gelu(jnp.dot(normed, wbuf[tt, 0], preferred_element_type=f32)))
        a = jax.nn.gelu(jnp.dot(normed, wbuf[tt, 1], preferred_element_type=f32))
        act.append(a)
        total = total + jnp.sum(a, axis=-1, keepdims=True)
        squares = squares + jnp.sum(a * a, axis=-1, keepdims=True)
    center = total / width
    spread = squares / width - center * center
    inv = lax.rsqrt(spread + epsilon)
    span = mkern.shape[1]
    causal = lax.broadcasted_iota(jnp.int32, (span, span), 0) >= lax.broadcasted_iota(
        jnp.int32, (span, span), 1
    )
    diagonal = lax.broadcasted_iota(jnp.int32, (span, span), 0) == lax.broadcasted_iota(
        jnp.int32, (span, span), 1
    )
    out = None
    for tt in range(n_tp):
        own = t ^ tt
        group = (own * lw) // cfg["group_ch"]
        values = (
            (act[tt] - center) * inv * lgain[own].astype(f32) + lshift[own].astype(f32)
        ).astype(bf16)
        kern = jnp.where(causal, mkern[group].astype(f32), 0.0).astype(bf16)
        offset = jnp.sum(jnp.where(diagonal, moff[group].astype(f32), 0.0), axis=1, keepdims=True)
        mixed = [
            jnp.dot(kern, values[i : i + span], preferred_element_type=f32) + offset
            for i in range(0, values.shape[0], span)
        ]
        mixed = mixed[0] if len(mixed) == 1 else jnp.concatenate(mixed, axis=0)
        gated = (gate_u[tt] * mixed).astype(bf16)
        term = contract_last(gated, wbuf[tt, 2])
        out = term if out is None else out + term
    middle = (x + out).astype(bf16)
    mid[...] = middle
    m = middle.astype(f32)
    scale2 = lax.rsqrt(jnp.mean(m * m, axis=-1, keepdims=True) + epsilon)
    normed2[...] = (m * scale2 * fgain[...].astype(f32)).astype(bf16)


def hidden_kernel(cfg, *refs):
    n = cfg["tokens"]
    tokens, weights = refs[:n], refs[n : n + len(cfg["weights"])]
    hid, wbuf, sem = refs[n + len(cfg["weights"]) :]
    k, r = lax.axis_index("fs"), lax.axis_index("rep")
    copies = []
    for i, (ref, (j, rr)) in enumerate(zip(weights, cfg["weights"])):
        base = (k ^ j) * cfg["rows"]
        if rr is not None:
            base = base + (r ^ rr) * cfg["part"]
        base = pl.multiple_of(base, cfg["part"])
        copies.append(pltpu.make_async_copy(ref, wbuf.at[pl.ds(base, ref.shape[0])], sem.at[i]))
    for c in copies:
        c.start()
    for c in copies:
        c.wait()
    half = hid.shape[1]
    start = 0
    for ref in tokens:
        pre = jnp.dot(ref[...], wbuf[...], preferred_element_type=f32)
        size = ref.shape[0]
        hid[start : start + size] = (jax.nn.silu(pre[:, :half]) * pre[:, half:]).astype(bf16)
        start += size


def down_kernel(packed, hid, *refs):
    weights, (keep, send) = refs[:-2], refs[-2:]
    half = hid.shape[1]
    top = keep.shape[0]
    col = 0
    h = hid[...]
    for ref in weights:
        for i in range(2 if packed else 1):
            w = ref[:, i * half : (i + 1) * half]
            res = contract_last(h, w).astype(bf16)
            keep[:, col : col + w.shape[0]] = res[:top]
            send[:, col : col + w.shape[0]] = res[top:]
            col += w.shape[0]


def per_device(
    sizes,
    tokens,
    mix_gain,
    gate_proj,
    value_proj,
    layer_gain,
    layer_shift,
    mix_kernel,
    mix_offset,
    out_proj,
    ffn_gain,
    ffn_gate,
    ffn_up,
    ffn_down,
):
    n_rep, n_fs, n_tp = sizes
    r, k = lax.axis_index("rep"), lax.axis_index("fs")
    b = k & 1
    count, d_model = tokens.shape
    rows, lw = gate_proj.shape
    part = rows // n_rep
    width = layer_gain.shape[0]
    ff = ffn_gate.shape[1]
    half = ff // 2
    any_spec = pl.BlockSpec(memory_space=pl.ANY)
    hbm_spec = pl.BlockSpec(memory_space=pltpu.HBM)
    vmem_spec = pl.BlockSpec(memory_space=pltpu.VMEM)
    far_first = list(range(n_fs - 1, 0, -1))

    pack, mine = pl.pallas_call(
        functools.partial(pack_kernel, part),
        out_shape=[
            jax.ShapeDtypeStruct((3, rows, lw), bf16),
            jax.ShapeDtypeStruct((3, part, lw), bf16),
        ],
        in_specs=[hbm_spec] * 3,
        out_specs=[vmem_spec] * 2,
        scratch_shapes=[pltpu.SemaphoreType.DMA((6,))],
        compiler_params=pltpu.CompilerParams(vmem_limit_bytes=4 * MIB),
        name="pack",
    )(gate_proj, value_proj, out_proj)
    got = {j: xor_permute(mine, "fs", j, n_fs) for j in far_first}

    def columns(w, which):
        return jnp.where(which == 0, w[:, :half], w[:, half:])

    def take_part(w, rr):
        return lax.dynamic_slice_in_dim(w, (r ^ rr) * part, part, axis=0)

    gate_up = jnp.concatenate([columns(ffn_gate, b), columns(ffn_up, b)], axis=1)
    g_part, u_part = take_part(ffn_gate, 0), take_part(ffn_up, 0)
    gu_same = jnp.concatenate([columns(g_part, b), columns(u_part, b)], axis=1)
    gu_other = jnp.concatenate([columns(g_part, 1 - b), columns(u_part, 1 - b)], axis=1)
    gu_z = {j: xor_permute(gu_other if j & 1 else gu_same, "fs", j, n_fs) for j in far_first}
    gu_weights, gu_where = [None], [(0, None)]
    for j in far_first:
        gu_weights.append(gu_z[j])
        gu_where.append((j, 0))
        for m in range(1, n_rep):
            gu_weights.append(xor_permute(gu_z[j], "rep", m, n_rep))
            gu_where.append((j, m))

    def fold(w):
        return jnp.concatenate([w[: part // 2], w[part // 2 :]], axis=1)

    down_own = jnp.concatenate([columns(take_part(ffn_down, m), b) for m in range(n_rep)], axis=0)
    d_part = take_part(ffn_down, 0)
    d_same, d_other = fold(columns(d_part, b)), fold(columns(d_part, 1 - b))

    def exchange(bundles, axis, m, n):
        arrays, segs, at = [], [], 0
        for array, entries in bundles:
            if axis == "rep":
                entries = [e for e in entries if e[3] is not None]
                if not entries:
                    continue
            arrays.append(array)
            for start, num, j, rr, tt in entries:
                if axis == "rep":
                    rr = rr ^ m
                else:
                    tt = tt ^ m
                segs.append((start + at, num, j, rr, tt))
            at += array.shape[1]
        joined = arrays[0] if len(arrays) == 1 else jnp.concatenate(arrays, axis=1)
        return (xor_permute(joined, axis, m, n), segs)

    smalls = (
        mix_gain[None],
        layer_gain.reshape(n_tp, 1, lw),
        layer_shift.reshape(n_tp, 1, lw),
        mix_offset[:, None, :],
        ffn_gain[None],
    )
    tied = lax.optimization_barrier((got[1], smalls, gate_up, down_own, d_same, d_other))
    got[1], smalls, gate_up, down_own, d_same, d_other = tied

    near = [(pack, [(0, rows, 0, None, 0)])]
    near += [(got[j], [(0, part, j, 0, 0)]) for j in range(1, n_fs // 2)]
    far = [(got[j], [(0, part, j, 0, 0)]) for j in range(n_fs // 2, n_fs)]
    steps = [("rep", m, n_rep) for m in bits(n_rep)] + [("tp", m, n_tp) for m in bits(n_tp, 2)]
    for step in steps:
        near.append(exchange(near, *step))
    for step in reversed(steps):
        far.append(exchange(far, *step))
    bundles = near + far
    for bundle in list(bundles):
        bundles.append(exchange([bundle], "tp", 1, n_tp))

    gu_weights[0] = gate_up
    segments = [segs for _, segs in bundles]
    cfg = dict(
        rows=rows,
        part=part,
        lw=lw,
        width=width,
        group_ch=width // mix_kernel.shape[0],
        segments=segments,
    )
    n_copies = sum(len(s) for s in segments)
    middle, normed2 = pl.pallas_call(
        functools.partial(mixer_kernel, cfg),
        out_shape=[jax.ShapeDtypeStruct((count, d_model), bf16)] * 2,
        in_specs=[vmem_spec] * 7 + [any_spec] * len(bundles),
        out_specs=[vmem_spec] * 2,
        scratch_shapes=[
            pltpu.VMEM((n_tp, 3, d_model, lw), bf16),
            pltpu.SemaphoreType.DMA((n_copies,)),
        ],
        compiler_params=pltpu.CompilerParams(vmem_limit_bytes=24 * MIB),
        cost_estimate=pl.CostEstimate(
            flops=6 * count * d_model * width,
            bytes_accessed=6 * d_model * width,
            transcendentals=2 * count * width,
        ),
        name="mixer",
    )(
        tokens,
        *smalls[:3],
        mix_kernel,
        *smalls[3:],
        *[array for array, _ in bundles],
    )

    ny = n_tp // 2
    h = count // 2
    col_a, col_b = normed2[:h], normed2[h:]
    col_a = jnp.concatenate([col_a, xor_permute(col_a, "fs", 1, n_fs)], axis=0)
    for m in bits(n_tp, 2):
        col_a = jnp.concatenate([col_a, xor_permute(col_a, "tp", m, n_tp)], axis=0)
        col_b = jnp.concatenate([col_b, xor_permute(col_b, "tp", m, n_tp)], axis=0)
    col_b = jnp.concatenate([col_b, xor_permute(col_b, "fs", 1, n_fs)], axis=0)
    groups = [col_a, col_b, xor_permute(col_a, "tp", 1, n_tp), xor_permute(col_b, "tp", 1, n_tp)]
    group_tokens = sum(g.shape[0] for g in groups)

    d_z = {j: xor_permute(d_other if j & 1 else d_same, "fs", j, n_fs) for j in far_first}
    d_x = {j: [xor_permute(d_z[j], "rep", m, n_rep) for m in range(1, n_rep)] for j in far_first}

    hidden = pl.pallas_call(
        functools.partial(
            hidden_kernel, dict(rows=rows, part=part, tokens=len(groups), weights=gu_where)
        ),
        out_shape=jax.ShapeDtypeStruct((group_tokens, half), bf16),
        in_specs=[vmem_spec] * len(groups) + [any_spec] * len(gu_weights),
        out_specs=vmem_spec,
        scratch_shapes=[
            pltpu.VMEM((d_model, ff), bf16),
            pltpu.SemaphoreType.DMA((len(gu_weights),)),
        ],
        compiler_params=pltpu.CompilerParams(vmem_limit_bytes=24 * MIB),
        cost_estimate=pl.CostEstimate(
            flops=2 * group_tokens * d_model * ff,
            bytes_accessed=2 * d_model * (group_tokens + ff),
            transcendentals=group_tokens * half,
        ),
        name="hidden",
    )(*groups, *gu_weights)

    def down(weights, packed):
        return pl.pallas_call(
            functools.partial(down_kernel, packed),
            out_shape=[jax.ShapeDtypeStruct((group_tokens // 2, rows), bf16)] * 2,
            in_specs=[vmem_spec] * (1 + len(weights)),
            out_specs=[vmem_spec] * 2,
            compiler_params=pltpu.CompilerParams(vmem_limit_bytes=12 * MIB),
            cost_estimate=pl.CostEstimate(
                flops=2 * group_tokens * half * rows,
                bytes_accessed=2 * group_tokens * (half + rows),
                transcendentals=0,
            ),
        )(hidden, *weights)

    def add(left, right):
        return (left.astype(f32) + right.astype(f32)).astype(bf16)

    kept, sent = {}, {}
    for j in range(n_fs):
        keep, send = down([d_z[j]] + d_x[j] if j else [down_own], j > 0)
        part_tokens = group_tokens // 2
        total = add(keep, xor_permute(send, "tp", 1, n_tp))
        left = total[: part_tokens // 2].reshape(ny, 2, h, rows)
        right = total[part_tokens // 2 :].reshape(2, ny, h, rows)
        for m in reversed(bits(n_tp, 2)):
            n = m // 2
            out_block = jnp.concatenate(
                [left[n:].reshape(-1, rows), right[:, n:].reshape(-1, rows)], axis=0
            )
            back = xor_permute(out_block, "tp", m, n_tp)
            mid_row = back.shape[0] // 2
            left = add(left[:n], back[:mid_row].reshape(n, 2, h, rows))
            right = add(right[:, :n], back[mid_row:].reshape(2, n, h, rows))
        kept[j] = jnp.concatenate([left[0, 0], right[0, 0]], axis=0)
        sent[j] = xor_permute(jnp.concatenate([left[0, 1], right[1, 0]], axis=0), "fs", 1, n_fs)
    pieces = []
    for j in range(n_fs):
        total = kept[j].astype(f32) + sent[j ^ 1].astype(f32)
        pieces.append(
            jnp.concatenate(
                absolute([total[:, m * part : (m + 1) * part] for m in range(n_rep)], r), axis=1
            )
        )
    summed = jnp.concatenate(absolute(pieces, k), axis=1)
    return (middle.astype(f32) + summed).astype(bf16)


def solution(mesh):
    token_spec = P(("rep", "fs", "tp"), None)
    weight_spec = P("fs", "tp")
    placed = (
        token_spec,
        P(),
        weight_spec,
        weight_spec,
        P(),
        P(),
        P(),
        P(),
        weight_spec,
        P(),
        weight_spec,
        weight_spec,
        weight_spec,
    )
    sizes = (mesh.shape["rep"], mesh.shape["fs"], mesh.shape["tp"])

    def body(*args):
        return per_device(sizes, *args)

    return jax.shard_map(
        body, mesh=mesh, in_specs=placed, out_specs=token_spec, check_vma=False
    )
```

profile of v0, /device:TPU:0, one launch (start us, length us, event | category | flops | bytes accessed | tf_op | source)
XLA Modules:
  0.0 257.4 jit_solution(14643222619383141898)
XLA Ops:
  3.5 3.1 %collective-permute-start = (bf16[3,256,128]{2,1,0:T(8,128)(2,1)S(1)}, bf16[3,256,128]{2,1,0:T(8,128)(2,1)S(1)}, u32[]{:S(2)}, u32[]{:S(2)}) collective-permute-start(bf16[3,256,128]{2,1,0:T(8,128)(2,1)S(1)} %get-tuple-element.27), channel_id=1, source_target_pairs={{0,4},{4,0},{8,12},{12,8},{1,5},{5,1},{9,13},{13,9},{2,6},{6,2},{1... | collective-permute-start | bytes 589832 | tf_op jit(solution)/shard_map/ppermute | solution.py:17
  6.6 2.6 %collective-permute-start.3 = (bf16[3,256,128]{2,1,0:T(8,128)(2,1)S(1)}, bf16[3,256,128]{2,1,0:T(8,128)(2,1)S(1)}, u32[]{:S(2)}, u32[]{:S(2)}) collective-permute-start(bf16[3,256,128]{2,1,0:T(8,128)(2,1)S(1)} %get-tuple-element.27), channel_id=1, source_target_pairs={{0,8},{4,12},{8,0},{12,4},{1,9},{5,13},{9,1},{13,5},{2,10},{6,14},... | collective-permute-start | bytes 589832 | tf_op jit(solution)/shard_map/ppermute | solution.py:17
  9.2 2.6 %broadcast_select_fusion.2 = (bf16[256,704]{1,0:T(8,128)(2,1)S(1)}, bf16[256,704]{1,0:T(8,128)(2,1)S(1)}, bf16[256,704]{1,0:T(8,128)(2,1)S(1)}, bf16[256,704]{1,0:T(8,128)(2,1)S(1)}, bf16[256,704]{1,0:T(8,128)(2,1)S(1)}) fusion(pred[]{:T(512)S(6)} %eq.5, bf16[512,1408]{1,0:T(8,128)(2,1)} %param.25, s32[]{:T(128)S(6)} %select_n.135, s32[]{:T(128)S(6)} %add.115, ...), kind=kLoop, calls=%fused_computation.22 | loop fusion | flops 901120 | bytes 3964942 | tf_op jit(solution)/shard_map/jit(_where)/select_n | solution.py:207
  14.5 9.3 %collective-permute-done.3.rest_4_ = bf16[3,256,128]{2,1,0:T(8,128)(2,1)S(1)} collective-permute-done((bf16[3,256,128]{2,1,0:T(8,128)(2,1)S(1)}, bf16[3,256,128]{2,1,0:T(8,128)(2,1)S(1)}, u32[]{:S(2)}, u32[]{:S(2)}) %collective-permute-start.3) | collective-permute-done | bytes 196640 | tf_op jit(solution)/shard_map/ppermute | solution.py:17
  27.0 4.2 %collective-permute-done.1.rest_2_ = bf16[3,256,128]{2,1,0:T(8,128)(2,1)S(1)} collective-permute-done((bf16[3,256,128]{2,1,0:T(8,128)(2,1)S(1)}, bf16[3,256,128]{2,1,0:T(8,128)(2,1)S(1)}, u32[]{:S(2)}, u32[]{:S(2)}) %collective-permute-start.1) | collective-permute-done | bytes 196640 | tf_op jit(solution)/shard_map/ppermute | solution.py:17
  31.9 2.7 %collective-permute-done.5.rest_6_ = bf16[3,512,128]{2,1,0:T(8,128)(2,1)S(1)} collective-permute-done((bf16[3,512,128]{2,1,0:T(8,128)(2,1)S(1)}, bf16[3,512,128]{2,1,0:T(8,128)(2,1)S(1)}, u32[]{:S(2)}, u32[]{:S(2)}) %collective-permute-start.5) | collective-permute-done | bytes 393248 | tf_op jit(solution)/shard_map/ppermute | solution.py:17
  36.2 12.9 %collective-permute-done.2.rest_3_ = bf16[3,1024,128]{2,1,0:T(8,128)(2,1)S(1)} collective-permute-done((bf16[3,1024,128]{2,1,0:T(8,128)(2,1)S(1)}, bf16[3,1024,128]{2,1,0:T(8,128)(2,1)S(1)}, u32[]{:S(2)}, u32[]{:S(2)}) %collective-permute-start.2) | collective-permute-done | bytes 786464 | tf_op jit(solution)/shard_map/ppermute | solution.py:17
  50.2 2.7 %collective-permute-done.8.rest_9_ = bf16[3,256,128]{2,1,0:T(8,128)(2,1)S(1)} collective-permute-done((bf16[3,256,128]{2,1,0:T(8,128)(2,1)S(1)}, bf16[3,256,128]{2,1,0:T(8,128)(2,1)S(1)}, u32[]{:S(2)}, u32[]{:S(2)}) %collective-permute-start.8) | collective-permute-done | bytes 196640 | tf_op jit(solution)/shard_map/ppermute | solution.py:17
  55.8 5.6 %mixer.1 = (bf16[128,2048]{1,0:T(8,128)(2,1)S(1)}, bf16[128,2048]{1,0:T(8,128)(2,1)S(1)}) custom-call(bf16[128,2048]{1,0:T(8,128)(2,1)S(1)} %copy-done, bf16[1,2048]{1,0:T(2,128)(2,1)S(1)} %broadcast_in_dim.9.gain, bf16[4,1,128]{2,1,0:T(2,128)(2,1)S(1)} %copy.18.lgain, bf16[4,1,128]{2,1,0:T(2,128)(2,1)S(1)} %copy.19.lshift, ...), custom_call_target="tpu_custom_call" | custom-call | flops 805306368 | bytes 6291456 | tf_op jit(solution)/shard_map/mixer/pallas_call | solution.py:283
  63.0 4.7 %collective-permute-start.15 = (bf16[64,2048]{1,0:T(8,128)(2,1)S(1)}, bf16[64,2048]{1,0:T(8,128)(2,1)S(1)}, u32[]{:S(2)}, u32[]{:S(2)}) collective-permute-start(bf16[64,2048]{1,0:T(8,128)(2,1)S(1)} %get-tuple-element.61), channel_id=1, source_target_pairs={{0,4},{4,0},{8,12},{12,8},{1,5},{5,1},{9,13},{13,9},{2,6},{6,2},{1... | collective-permute-start | bytes 786440 | tf_op jit(solution)/shard_map/ppermute | solution.py:17
  69.9 4.8 %collective-permute-start.18 = (bf16[128,2048]{1,0:T(8,128)(2,1)S(1)}, bf16[128,2048]{1,0:T(8,128)(2,1)S(1)}, u32[]{:S(2)}, u32[]{:S(2)}) collective-permute-start(bf16[128,2048]{1,0:T(8,128)(2,1)S(1)} %pad_maximum_fusion.9), channel_id=1, source_target_pairs={{0,4},{4,0},{8,12},{12,8},{1,5},{5,1},{9,13},{13,9},{2,6},{6,2},{1... | collective-permute-start | bytes 1572872 | tf_op jit(solution)/shard_map/ppermute | solution.py:17
  76.5 2.5 collective-permute-start.21
  79.3 2.0 collective-permute-start.23
  81.3 7.1 %collective-permute-done.18 = bf16[128,2048]{1,0:T(8,128)(2,1)S(1)} collective-permute-done((bf16[128,2048]{1,0:T(8,128)(2,1)S(1)}, bf16[128,2048]{1,0:T(8,128)(2,1)S(1)}, u32[]{:S(2)}, u32[]{:S(2)}) %collective-permute-start.18) | collective-permute-done | bytes 524320 | tf_op jit(solution)/shard_map/ppermute | solution.py:17
  89.8 50.3 %collective-permute-done.37.refs_0_ = bf16[128,1408]{1,0:T(8,128)(2,1)S(1)} collective-permute-done((bf16[128,1408]{1,0:T(8,128)(2,1)S(1)}, bf16[128,1408]{1,0:T(8,128)(2,1)S(1)}, u32[]{:S(2)}, u32[]{:S(2)}) %collective-permute-start.37) | collective-permute-done | bytes 360480 | tf_op jit(solution)/shard_map/ppermute | solution.py:17
  143.6 15.5 %collective-permute-done.22.refs_6_ = bf16[256,1408]{1,0:T(8,128)(2,1)S(1)} collective-permute-done((bf16[256,1408]{1,0:T(8,128)(2,1)S(1)}, bf16[256,1408]{1,0:T(8,128)(2,1)S(1)}, u32[]{:S(2)}, u32[]{:S(2)}) %collective-permute-start.22) | collective-permute-done | bytes 720928 | tf_op jit(solution)/shard_map/ppermute | solution.py:17
  159.1 2.5 collective-permute-start.27
  161.6 13.0 %collective-permute-done.26.refs_10_ = bf16[256,1408]{1,0:T(8,128)(2,1)S(1)} collective-permute-done((bf16[256,1408]{1,0:T(8,128)(2,1)S(1)}, bf16[256,1408]{1,0:T(8,128)(2,1)S(1)}, u32[]{:S(2)}, u32[]{:S(2)}) %collective-permute-start.26) | collective-permute-done | bytes 720928 | tf_op jit(solution)/shard_map/ppermute | solution.py:17
  174.6 2.8 %collective-permute-start.31 = (bf16[128,1408]{1,0:T(8,128)(2,1)S(1)}, bf16[128,1408]{1,0:T(8,128)(2,1)S(1)}, u32[]{:S(2)}, u32[]{:S(2)}) collective-permute-start(bf16[128,1408]{1,0:T(8,128)(2,1)S(1)} %pad_maximum_fusion.11), channel_id=1, source_target_pairs={{0,8},{4,12},{8,0},{12,4},{1,9},{5,13},{9,1},{13,5},{2,10},{6,14},... | collective-permute-start | bytes 1081352 | tf_op jit(solution)/shard_map/ppermute | solution.py:17
  177.4 12.2 %collective-permute-done.24.refs_8_ = bf16[256,1408]{1,0:T(8,128)(2,1)S(1)} collective-permute-done((bf16[256,1408]{1,0:T(8,128)(2,1)S(1)}, bf16[256,1408]{1,0:T(8,128)(2,1)S(1)}, u32[]{:S(2)}, u32[]{:S(2)}) %collective-permute-start.24) | collective-permute-done | bytes 720928 | tf_op jit(solution)/shard_map/ppermute | solution.py:17
  191.1 9.1 %hidden.1.hid = bf16[1024,704]{1,0:T(8,128)(2,1)S(1)} custom-call(bf16[256,2048]{1,0:T(8,128)(2,1)S(1)} %pad_maximum_fusion.1.refs_0_, bf16[256,2048]{1,0:T(8,128)(2,1)S(1)} %pad_maximum_fusion.2.refs_1_, bf16[256,2048]{1,0:T(8,128)(2,1)S(1)} %collective-permute-done.19.refs_2_, bf16[256,2048]{1,0:T(8,128)(2,1)S(1)} %collective-permute-done.20.refs_3_, ...), custom_call_target="tpu_custom_call" | custom-call | flops 5905580032 | bytes 9961472 | tf_op jit(solution)/shard_map/hidden/pallas_call | solution.py:321
  205.3 7.4 %collective-permute-done.32.refs_1_ = bf16[128,1408]{1,0:T(8,128)(2,1)} collective-permute-done((bf16[128,1408]{1,0:T(8,128)(2,1)S(1)}, bf16[128,1408]{1,0:T(8,128)(2,1)}, u32[]{:S(2)}, u32[]{:S(2)}) %collective-permute-start.32) | collective-permute-done | bytes 360480 | tf_op jit(solution)/shard_map/ppermute | solution.py:17
  214.1 2.8 %shard_map.128 = (bf16[512,512]{1,0:T(8,128)(2,1)S(1)}, bf16[512,512]{1,0:T(8,128)(2,1)S(1)}) custom-call(bf16[1024,704]{1,0:T(8,128)(2,1)S(1)} %copy-done.6, bf16[128,1408]{1,0:T(8,128)(2,1)S(1)} %collective-permute-done.31.refs_0_, bf16[128,1408]{1,0:T(8,128)(2,1)} %collective-permute-done.32.refs_1_), custom_call_target="tpu_custom_call" | custom-call | flops 738197504 | bytes 2490368 | tf_op jit(solution)/shard_map/pallas_call | solution.py:342
  217.0 2.9 %collective-permute-done.28.refs_1_ = bf16[128,1408]{1,0:T(8,128)(2,1)} collective-permute-done((bf16[128,1408]{1,0:T(8,128)(2,1)S(1)}, bf16[128,1408]{1,0:T(8,128)(2,1)}, u32[]{:S(2)}, u32[]{:S(2)}) %collective-permute-start.28) | collective-permute-done | bytes 360480 | tf_op jit(solution)/shard_map/ppermute | solution.py:17
  219.9 2.8 %shard_map.127 = (bf16[512,512]{1,0:T(8,128)(2,1)S(1)}, bf16[512,512]{1,0:T(8,128)(2,1)S(1)}) custom-call(bf16[1024,704]{1,0:T(8,128)(2,1)S(1)} %copy-done.6, bf16[128,1408]{1,0:T(8,128)(2,1)S(1)} %collective-permute-done.27.refs_0_, bf16[128,1408]{1,0:T(8,128)(2,1)} %collective-permute-done.28.refs_1_), custom_call_target="tpu_custom_call" | custom-call | flops 738197504 | bytes 2490368 | tf_op jit(solution)/shard_map/pallas_call | solution.py:342
  230.9 3.6 %collective-permute-done.42 = bf16[256,512]{1,0:T(8,128)(2,1)S(1)} collective-permute-done((bf16[256,512]{1,0:T(8,128)(2,1)S(1)}, bf16[256,512]{1,0:T(8,128)(2,1)S(1)}, u32[]{:S(2)}, u32[]{:S(2)}) %collective-permute-start.42) | collective-permute-done | bytes 262176 | tf_op jit(solution)/shard_map/ppermute | solution.py:17
  234.7 1.9 collective-permute-start.43
  236.6 3.6 %collective-permute-done.40 = bf16[256,512]{1,0:T(8,128)(2,1)S(1)} collective-permute-done((bf16[256,512]{1,0:T(8,128)(2,1)S(1)}, bf16[256,512]{1,0:T(8,128)(2,1)S(1)}, u32[]{:S(2)}, u32[]{:S(2)}) %collective-permute-start.40) | collective-permute-done | bytes 262176 | tf_op jit(solution)/shard_map/ppermute | solution.py:17
  242.2 3.6 %collective-permute-done.34 = bf16[256,512]{1,0:T(8,128)(2,1)S(1)} collective-permute-done((bf16[256,512]{1,0:T(8,128)(2,1)S(1)}, bf16[256,512]{1,0:T(8,128)(2,1)S(1)}, u32[]{:S(2)}, u32[]{:S(2)}) %collective-permute-start.34) | collective-permute-done | bytes 262176 | tf_op jit(solution)/shard_map/ppermute | solution.py:17
  245.9 1.9 collective-permute-start.35
  247.8 3.1 %collective-permute-done.30 = bf16[256,512]{1,0:T(8,128)(2,1)S(1)} collective-permute-done((bf16[256,512]{1,0:T(8,128)(2,1)S(1)}, bf16[256,512]{1,0:T(8,128)(2,1)S(1)}, u32[]{:S(2)}, u32[]{:S(2)}) %collective-permute-start.30) | collective-permute-done | bytes 262176 | tf_op jit(solution)/shard_map/ppermute | solution.py:17
  253.2 3.1 %collective-permute-done.36 = bf16[128,512]{1,0:T(8,128)(2,1)S(1)} collective-permute-done((bf16[128,512]{1,0:T(8,128)(2,1)S(1)}, bf16[128,512]{1,0:T(8,128)(2,1)S(1)}, u32[]{:S(2)}, u32[]{:S(2)}) %collective-permute-start.36) | collective-permute-done | bytes 131104 | tf_op jit(solution)/shard_map/ppermute | solution.py:17
  (177 shorter events, 47.8 us)
Async XLA Ops:
  3.5 22.0 %collective-permute-start = (bf16[3,256,128]{2,1,0:T(8,128)(2,1)S(1)}, bf16[3,256,128]{2,1,0:T(8,128)(2,1)S(1)}, u32[]{:S(2)}, u32[]{:S(2)}) collective-permute-start(bf16[3,256,128]{2,1,0:T(8,128)(2,1)S(1)} %get-tuple-element.27), channel_id=1, source_target_pairs={{0,4},{4,0},{8,12},{12,8},{1,5},{5,1},{9,13},{13,9},{2,6},{6,2},{1... | collective-permute-start | bytes 589832 | tf_op jit(solution)/shard_map/ppermute | solution.py:17
  6.6 17.1 %collective-permute-start.3 = (bf16[3,256,128]{2,1,0:T(8,128)(2,1)S(1)}, bf16[3,256,128]{2,1,0:T(8,128)(2,1)S(1)}, u32[]{:S(2)}, u32[]{:S(2)}) collective-permute-start(bf16[3,256,128]{2,1,0:T(8,128)(2,1)S(1)} %get-tuple-element.27), channel_id=1, source_target_pairs={{0,8},{4,12},{8,0},{12,4},{1,9},{5,13},{9,1},{13,5},{2,10},{6,14},... | collective-permute-start | bytes 589832 | tf_op jit(solution)/shard_map/ppermute | solution.py:17
  9.2 14.5 %collective-permute-start.4 = (bf16[3,256,128]{2,1,0:T(8,128)(2,1)S(1)}, bf16[3,256,128]{2,1,0:T(8,128)(2,1)S(1)}, u32[]{:S(2)}, u32[]{:S(2)}) collective-permute-start(bf16[3,256,128]{2,1,0:T(8,128)(2,1)S(1)} %get-tuple-element.27), channel_id=1, source_target_pairs={{0,12},{4,8},{8,4},{12,0},{1,13},{5,9},{9,5},{13,1},{2,14},{6,10},... | collective-permute-start | bytes 589832 | tf_op jit(solution)/shard_map/ppermute | solution.py:17
  23.8 10.8 %collective-permute-start.5 = (bf16[3,512,128]{2,1,0:T(8,128)(2,1)S(1)}, bf16[3,512,128]{2,1,0:T(8,128)(2,1)S(1)}, u32[]{:S(2)}, u32[]{:S(2)}) collective-permute-start(bf16[3,512,128]{2,1,0:T(8,128)(2,1)S(1)} %pad_maximum_fusion.10), channel_id=1, source_target_pairs={{0,2},{1,3},{2,0},{3,1},{4,6},{5,7},{6,4},{7,5},{8,10},{9,11},{10,... | collective-permute-start | bytes 1179656 | tf_op jit(solution)/shard_map/ppermute | solution.py:17
  31.3 17.8 %collective-permute-start.2 = (bf16[3,1024,128]{2,1,0:T(8,128)(2,1)S(1)}, bf16[3,1024,128]{2,1,0:T(8,128)(2,1)S(1)}, u32[]{:S(2)}, u32[]{:S(2)}) collective-permute-start(bf16[3,1024,128]{2,1,0:T(8,128)(2,1)S(1)} %pad_maximum_fusion.4), channel_id=1, source_target_pairs={{0,2},{1,3},{2,0},{3,1},{4,6},{5,7},{6,4},{7,5},{8,10},{9,11},{10,... | collective-permute-start | bytes 2359304 | tf_op jit(solution)/shard_map/ppermute | solution.py:17
  34.6 14.5 %collective-permute-start.6 = (bf16[3,1024,128]{2,1,0:T(8,128)(2,1)S(1)}, bf16[3,1024,128]{2,1,0:T(8,128)(2,1)S(1)}, u32[]{:S(2)}, u32[]{:S(2)}) collective-permute-start(bf16[3,1024,128]{2,1,0:T(8,128)(2,1)S(1)} %pad_maximum_fusion.5), channel_id=1, source_target_pairs={{0,16},{16,0},{1,17},{17,1},{2,18},{18,2},{3,19},{19,3},{4,20},{20... | collective-permute-start | bytes 2359304 | tf_op jit(solution)/shard_map/ppermute | solution.py:17
  63.0 11.7 %collective-permute-start.15 = (bf16[64,2048]{1,0:T(8,128)(2,1)S(1)}, bf16[64,2048]{1,0:T(8,128)(2,1)S(1)}, u32[]{:S(2)}, u32[]{:S(2)}) collective-permute-start(bf16[64,2048]{1,0:T(8,128)(2,1)S(1)} %get-tuple-element.61), channel_id=1, source_target_pairs={{0,4},{4,0},{8,12},{12,8},{1,5},{5,1},{9,13},{13,9},{2,6},{6,2},{1... | collective-permute-start | bytes 786440 | tf_op jit(solution)/shard_map/ppermute | solution.py:17
  69.9 18.5 %collective-permute-start.18 = (bf16[128,2048]{1,0:T(8,128)(2,1)S(1)}, bf16[128,2048]{1,0:T(8,128)(2,1)S(1)}, u32[]{:S(2)}, u32[]{:S(2)}) collective-permute-start(bf16[128,2048]{1,0:T(8,128)(2,1)S(1)} %pad_maximum_fusion.9), channel_id=1, source_target_pairs={{0,4},{4,0},{8,12},{12,8},{1,5},{5,1},{9,13},{13,9},{2,6},{6,2},{1... | collective-permute-start | bytes 1572872 | tf_op jit(solution)/shard_map/ppermute | solution.py:17
  74.7 14.9 %collective-permute-start.16 = (bf16[128,2048]{1,0:T(8,128)(2,1)S(1)}, bf16[128,2048]{1,0:T(8,128)(2,1)S(1)}, u32[]{:S(2)}, u32[]{:S(2)}) collective-permute-start(bf16[128,2048]{1,0:T(8,128)(2,1)S(1)} %pad_maximum_fusion.8), channel_id=1, source_target_pairs={{0,2},{1,3},{2,0},{3,1},{4,6},{5,7},{6,4},{7,5},{8,10},{9,11},{10,... | collective-permute-start | bytes 1572872 | tf_op jit(solution)/shard_map/ppermute | solution.py:17
  76.5 63.6 %collective-permute-start.21 = (bf16[256,1408]{1,0:T(8,128)(2,1)S(1)}, bf16[256,1408]{1,0:T(8,128)(2,1)S(1)}, u32[]{:S(2)}, u32[]{:S(2)}) collective-permute-start(bf16[256,1408]{1,0:T(8,128)(2,1)S(1)} %pad_maximum_fusion.6), channel_id=1, source_target_pairs={{0,12},{4,8},{8,4},{12,0},{1,13},{5,9},{9,5},{13,1},{2,14},{6,10},... | collective-permute-start | bytes 2162696 | tf_op jit(solution)/shard_map/ppermute | solution.py:17
  79.1 62.5 %collective-permute-start.25 = (bf16[256,1408]{1,0:T(8,128)(2,1)S(1)}, bf16[256,1408]{1,0:T(8,128)(2,1)S(1)}, u32[]{:S(2)}, u32[]{:S(2)}) collective-permute-start(bf16[256,1408]{1,0:T(8,128)(2,1)S(1)} %pad_maximum_fusion.6), channel_id=1, source_target_pairs={{0,4},{4,0},{8,12},{12,8},{1,5},{5,1},{9,13},{13,9},{2,6},{6,2},{1... | collective-permute-start | bytes 2162696 | tf_op jit(solution)/shard_map/ppermute | solution.py:17
  79.3 62.9 %collective-permute-start.23 = (bf16[256,1408]{1,0:T(8,128)(2,1)S(1)}, bf16[256,1408]{1,0:T(8,128)(2,1)S(1)}, u32[]{:S(2)}, u32[]{:S(2)}) collective-permute-start(bf16[256,1408]{1,0:T(8,128)(2,1)S(1)} %pad_maximum_fusion.7), channel_id=1, source_target_pairs={{0,8},{4,12},{8,0},{12,4},{1,9},{5,13},{9,1},{13,5},{2,10},{6,14},... | collective-permute-start | bytes 2162696 | tf_op jit(solution)/shard_map/ppermute | solution.py:17
  88.4 51.8 %collective-permute-start.37 = (bf16[128,1408]{1,0:T(8,128)(2,1)S(1)}, bf16[128,1408]{1,0:T(8,128)(2,1)S(1)}, u32[]{:S(2)}, u32[]{:S(2)}) collective-permute-start(bf16[128,1408]{1,0:T(8,128)(2,1)S(1)} %pad_maximum_fusion.12), channel_id=1, source_target_pairs={{0,4},{4,0},{8,12},{12,8},{1,5},{5,1},{9,13},{13,9},{2,6},{6,2},{1... | collective-permute-start | bytes 1081352 | tf_op jit(solution)/shard_map/ppermute | solution.py:17
  89.6 101.5 %collective-permute-start.20 = (bf16[256,2048]{1,0:T(8,128)(2,1)S(1)}, bf16[256,2048]{1,0:T(8,128)(2,1)S(1)}, u32[]{:S(2)}, u32[]{:S(2)}) collective-permute-start(bf16[256,2048]{1,0:T(8,128)(2,1)S(1)} %pad_maximum_fusion.2.refs_1_), channel_id=1, source_target_pairs={{0,1},{1,0},{2,3},{3,2},{4,5},{5,4},{6,7},{7,6},{8,9},{9,8},{10,11... | collective-permute-start | bytes 3145736 | tf_op jit(solution)/shard_map/ppermute | solution.py:17
  140.1 50.9 %collective-permute-start.19 = (bf16[256,2048]{1,0:T(8,128)(2,1)S(1)}, bf16[256,2048]{1,0:T(8,128)(2,1)S(1)}, u32[]{:S(2)}, u32[]{:S(2)}) collective-permute-start(bf16[256,2048]{1,0:T(8,128)(2,1)S(1)} %pad_maximum_fusion.1.refs_0_), channel_id=1, source_target_pairs={{0,1},{1,0},{2,3},{3,2},{4,5},{5,4},{6,7},{7,6},{8,9},{9,8},{10,11... | collective-permute-start | bytes 3145736 | tf_op jit(solution)/shard_map/ppermute | solution.py:17
  140.1 19.0 %collective-permute-start.22 = (bf16[256,1408]{1,0:T(8,128)(2,1)S(1)}, bf16[256,1408]{1,0:T(8,128)(2,1)S(1)}, u32[]{:S(2)}, u32[]{:S(2)}) collective-permute-start(bf16[256,1408]{1,0:T(8,128)(2,1)S(1)} %collective-permute-done.21.refs_5_), channel_id=1, source_target_pairs={{0,16},{16,0},{1,17},{17,1},{2,18},{18,2},{3,19},{19,3},{4,20},{20... | collective-permute-start | bytes 2162696 | tf_op jit(solution)/shard_map/ppermute | solution.py:17
  141.6 33.0 %collective-permute-start.26 = (bf16[256,1408]{1,0:T(8,128)(2,1)S(1)}, bf16[256,1408]{1,0:T(8,128)(2,1)S(1)}, u32[]{:S(2)}, u32[]{:S(2)}) collective-permute-start(bf16[256,1408]{1,0:T(8,128)(2,1)S(1)} %collective-permute-done.25.refs_9_), channel_id=1, source_target_pairs={{0,16},{16,0},{1,17},{17,1},{2,18},{18,2},{3,19},{19,3},{4,20},{20... | collective-permute-start | bytes 2162696 | tf_op jit(solution)/shard_map/ppermute | solution.py:17
  142.2 47.4 %collective-permute-start.24 = (bf16[256,1408]{1,0:T(8,128)(2,1)S(1)}, bf16[256,1408]{1,0:T(8,128)(2,1)S(1)}, u32[]{:S(2)}, u32[]{:S(2)}) collective-permute-start(bf16[256,1408]{1,0:T(8,128)(2,1)S(1)} %collective-permute-done.23.refs_7_), channel_id=1, source_target_pairs={{0,16},{16,0},{1,17},{17,1},{2,18},{18,2},{3,19},{19,3},{4,20},{20... | collective-permute-start | bytes 2162696 | tf_op jit(solution)/shard_map/ppermute | solution.py:17
  159.1 42.7 %collective-permute-start.27 = (bf16[128,1408]{1,0:T(8,128)(2,1)S(1)}, bf16[128,1408]{1,0:T(8,128)(2,1)S(1)}, u32[]{:S(2)}, u32[]{:S(2)}) collective-permute-start(bf16[128,1408]{1,0:T(8,128)(2,1)S(1)} %pad_maximum_fusion.12), channel_id=1, source_target_pairs={{0,12},{4,8},{8,4},{12,0},{1,13},{5,9},{9,5},{13,1},{2,14},{6,10},... | collective-permute-start | bytes 1081352 | tf_op jit(solution)/shard_map/ppermute | solution.py:17
  174.6 26.6 %collective-permute-start.31 = (bf16[128,1408]{1,0:T(8,128)(2,1)S(1)}, bf16[128,1408]{1,0:T(8,128)(2,1)S(1)}, u32[]{:S(2)}, u32[]{:S(2)}) collective-permute-start(bf16[128,1408]{1,0:T(8,128)(2,1)S(1)} %pad_maximum_fusion.11), channel_id=1, source_target_pairs={{0,8},{4,12},{8,0},{12,4},{1,9},{5,13},{9,1},{13,5},{2,10},{6,14},... | collective-permute-start | bytes 1081352 | tf_op jit(solution)/shard_map/ppermute | solution.py:17
  189.6 13.8 %collective-permute-start.38 = (bf16[128,1408]{1,0:T(8,128)(2,1)S(1)}, bf16[128,1408]{1,0:T(8,128)(2,1)S(1)}, u32[]{:S(2)}, u32[]{:S(2)}) collective-permute-start(bf16[128,1408]{1,0:T(8,128)(2,1)S(1)} %collective-permute-done.37.refs_0_), channel_id=1, source_target_pairs={{0,16},{16,0},{1,17},{17,1},{2,18},{18,2},{3,19},{19,3},{4,20},{20... | collective-permute-start | bytes 1081352 | tf_op jit(solution)/shard_map/ppermute | solution.py:17
  201.2 21.6 %collective-permute-start.41 = (bf16[512,512]{1,0:T(8,128)(2,1)S(1)}, bf16[512,512]{1,0:T(8,128)(2,1)}, u32[]{:S(2)}, u32[]{:S(2)}) collective-permute-start(bf16[512,512]{1,0:T(8,128)(2,1)S(1)} %get-tuple-element.48), channel_id=1, source_target_pairs={{0,1},{1,0},{2,3},{3,2},{4,5},{5,4},{6,7},{7,6},{8,9},{9,8},{10,11... | collective-permute-start | bytes 1572872 | tf_op jit(solution)/shard_map/ppermute | solution.py:17
  201.3 11.5 %collective-permute-start.32 = (bf16[128,1408]{1,0:T(8,128)(2,1)S(1)}, bf16[128,1408]{1,0:T(8,128)(2,1)}, u32[]{:S(2)}, u32[]{:S(2)}) collective-permute-start(bf16[128,1408]{1,0:T(8,128)(2,1)S(1)} %collective-permute-done.31.refs_0_), channel_id=1, source_target_pairs={{0,16},{16,0},{1,17},{17,1},{2,18},{18,2},{3,19},{19,3},{4,20},{20... | collective-permute-start | bytes 1081352 | tf_op jit(solution)/shard_map/ppermute | solution.py:17
  201.9 18.0 %collective-permute-start.28 = (bf16[128,1408]{1,0:T(8,128)(2,1)S(1)}, bf16[128,1408]{1,0:T(8,128)(2,1)}, u32[]{:S(2)}, u32[]{:S(2)}) collective-permute-start(bf16[128,1408]{1,0:T(8,128)(2,1)S(1)} %collective-permute-done.27.refs_0_), channel_id=1, source_target_pairs={{0,16},{16,0},{1,17},{17,1},{2,18},{18,2},{3,19},{19,3},{4,20},{20... | collective-permute-start | bytes 1081352 | tf_op jit(solution)/shard_map/ppermute | solution.py:17
  205.2 18.8 %collective-permute-start.39 = (bf16[512,512]{1,0:T(8,128)(2,1)S(1)}, bf16[512,512]{1,0:T(8,128)(2,1)}, u32[]{:S(2)}, u32[]{:S(2)}) collective-permute-start(bf16[512,512]{1,0:T(8,128)(2,1)S(1)} %get-tuple-element.45), channel_id=1, source_target_pairs={{0,1},{1,0},{2,3},{3,2},{4,5},{5,4},{6,7},{7,6},{8,9},{9,8},{10,11... | collective-permute-start | bytes 1572872 | tf_op jit(solution)/shard_map/ppermute | solution.py:17
  216.9 10.0 %collective-permute-start.33 = (bf16[512,512]{1,0:T(8,128)(2,1)S(1)}, bf16[512,512]{1,0:T(8,128)(2,1)S(1)}, u32[]{:S(2)}, u32[]{:S(2)}) collective-permute-start(bf16[512,512]{1,0:T(8,128)(2,1)S(1)} %get-tuple-element.43), channel_id=1, source_target_pairs={{0,1},{1,0},{2,3},{3,2},{4,5},{5,4},{6,7},{7,6},{8,9},{9,8},{10,11... | collective-permute-start | bytes 1572872 | tf_op jit(solution)/shard_map/ppermute | solution.py:17
  225.3 9.2 %collective-permute-start.42 = (bf16[256,512]{1,0:T(8,128)(2,1)S(1)}, bf16[256,512]{1,0:T(8,128)(2,1)S(1)}, u32[]{:S(2)}, u32[]{:S(2)}) collective-permute-start(bf16[256,512]{1,0:T(8,128)(2,1)S(1)} %pad_maximum_fusion.18), channel_id=1, source_target_pairs={{0,2},{1,3},{2,0},{3,1},{4,6},{5,7},{6,4},{7,5},{8,10},{9,11},{10,... | collective-permute-start | bytes 786440 | tf_op jit(solution)/shard_map/ppermute | solution.py:17
  228.1 12.1 %collective-permute-start.40 = (bf16[256,512]{1,0:T(8,128)(2,1)S(1)}, bf16[256,512]{1,0:T(8,128)(2,1)S(1)}, u32[]{:S(2)}, u32[]{:S(2)}) collective-permute-start(bf16[256,512]{1,0:T(8,128)(2,1)S(1)} %pad_maximum_fusion.17), channel_id=1, source_target_pairs={{0,2},{1,3},{2,0},{3,1},{4,6},{5,7},{6,4},{7,5},{8,10},{9,11},{10,... | collective-permute-start | bytes 786440 | tf_op jit(solution)/shard_map/ppermute | solution.py:17
  228.7 17.1 %collective-permute-start.34 = (bf16[256,512]{1,0:T(8,128)(2,1)S(1)}, bf16[256,512]{1,0:T(8,128)(2,1)S(1)}, u32[]{:S(2)}, u32[]{:S(2)}) collective-permute-start(bf16[256,512]{1,0:T(8,128)(2,1)S(1)} %pad_maximum_fusion.14), channel_id=1, source_target_pairs={{0,2},{1,3},{2,0},{3,1},{4,6},{5,7},{6,4},{7,5},{8,10},{9,11},{10,... | collective-permute-start | bytes 786440 | tf_op jit(solution)/shard_map/ppermute | solution.py:17
  230.4 20.6 %collective-permute-start.30 = (bf16[256,512]{1,0:T(8,128)(2,1)S(1)}, bf16[256,512]{1,0:T(8,128)(2,1)S(1)}, u32[]{:S(2)}, u32[]{:S(2)}) collective-permute-start(bf16[256,512]{1,0:T(8,128)(2,1)S(1)} %pad_maximum_fusion.13), channel_id=1, source_target_pairs={{0,2},{1,3},{2,0},{3,1},{4,6},{5,7},{6,4},{7,5},{8,10},{9,11},{10,... | collective-permute-start | bytes 786440 | tf_op jit(solution)/shard_map/ppermute | solution.py:17
  234.7 18.3 %collective-permute-start.43 = (bf16[128,512]{1,0:T(8,128)(2,1)S(1)}, bf16[128,512]{1,0:T(8,128)(2,1)S(1)}, u32[]{:S(2)}, u32[]{:S(2)}) collective-permute-start(bf16[128,512]{1,0:T(8,128)(2,1)S(1)} %pad_maximum_fusion.23), channel_id=1, source_target_pairs={{0,4},{4,0},{8,12},{12,8},{1,5},{5,1},{9,13},{13,9},{2,6},{6,2},{1... | collective-permute-start | bytes 393224 | tf_op jit(solution)/shard_map/ppermute | solution.py:17
  240.3 12.7 %collective-permute-start.44 = (bf16[128,512]{1,0:T(8,128)(2,1)S(1)}, bf16[128,512]{1,0:T(8,128)(2,1)S(1)}, u32[]{:S(2)}, u32[]{:S(2)}) collective-permute-start(bf16[128,512]{1,0:T(8,128)(2,1)S(1)} %pad_maximum_fusion.24), channel_id=1, source_target_pairs={{0,4},{4,0},{8,12},{12,8},{1,5},{5,1},{9,13},{13,9},{2,6},{6,2},{1... | collective-permute-start | bytes 393224 | tf_op jit(solution)/shard_map/ppermute | solution.py:17
  (30 other events, 228.8 us)
where the time goes:
time: 258 us; the launch traced here: 257 us
  waiting for transfers between devices  161 us (62%)
  starting transfers between devices  55.4 us (21%)
  Pallas kernels  24 us (9%)
  other arithmetic  9.3 us (4%)
  local copies, waits for them, and re-layouts  6.61 us (3%)
    ppermute x45, waiting for transfers between devices, xor_permute(): return lax.ppermute(x, axis, [(i, i ^ m) for i in range(n)])  161 us
    ppermute x45, starting transfers between devices, xor_permute(): return lax.ppermute(x, axis, [(i, i ^ m) for i in range(n)])  55.4 us
    pallas_call x1, Pallas kernels, per_device(): pl.pallas_call(functools.partial(hidden_kernel, dict(rows=rows, part=part...  9.07 us
    pallas_call x4, Pallas kernels, down(): pl.pallas_call(functools.partial(down_kernel, packed), out_shape=[jax.Sha...  8.5 us
    pallas_call x1, Pallas kernels, per_device(): pl.pallas_call(functools.partial(mixer_kernel, cfg), out_shape=[jax.Shape...  5.63 us
    unnamed x32, local copies, waits for them, and re-layouts  5.45 us
  transfers between devices with their start and end apart: 45, of which 21 were waited for; matrix products, arithmetic and copies ran while one was open for 3% of the time, Pallas kernels for 7%

commit v1 on v0

v1 whole, which is shorter than its diff:
```python
import functools

import jax
import jax.numpy as jnp
from jax import lax
from jax.experimental import pallas as pl
from jax.experimental.pallas import tpu as pltpu
from jax.sharding import PartitionSpec as P


epsilon = 1e-06
f32, bf16 = jnp.float32, jnp.bfloat16
MIB = 1024 * 1024


def xor_permute(x, axis, m, n):
    return lax.ppermute(x, axis, [(i, i ^ m) for i in range(n)])


def bits(n, low=1):
    out = []
    while low < n:
        out.append(low)
        low *= 2
    return out


def absolute(items, me):
    items = list(items)
    for m in bits(len(items)):
        flip = (me & m) != 0
        items = [jnp.where(flip, items[i ^ m], items[i]) for i in range(len(items))]
    return items


def contract_last(left, right):
    return lax.dot_general(left, right, (((1,), (1,)), ((), ())), preferred_element_type=f32)


def pack_kernel(part, *refs):
    weights, (full, mine, sem) = refs[:-3], refs[-3:]
    base = pl.multiple_of(lax.axis_index("rep") * part, part)
    copies = []
    for i, ref in enumerate(weights):
        copies.append(
            pltpu.make_async_copy(ref.at[pl.ds(base, part)], mine.at[i], sem.at[len(copies)])
        )
        copies.append(pltpu.make_async_copy(ref, full.at[i], sem.at[len(copies)]))
    for c in copies:
        c.start()
    for c in copies:
        c.wait()


def fetch(pairs, sem):
    copies = [pltpu.make_async_copy(a, b, sem.at[i]) for i, (a, b) in enumerate(pairs)]
    for c in copies:
        c.start()
    for c in copies:
        c.wait()


def send_kernel(part, gate, up, same, other, g, u, sem):
    at = pl.ds(pl.multiple_of(lax.axis_index("rep") * part, part), part)
    fetch([(gate.at[at], g), (up.at[at], u)], sem)
    half = gate.shape[1] // 2
    b = lax.axis_index("fs") & 1
    for case in range(2):

        @pl.when(b == case)
        def _():
            for ref, side in ((same, case), (other, 1 - case)):
                cut = slice(side * half, (side + 1) * half)
                ref[...] = jnp.concatenate([g[:, cut], u[:, cut]], axis=1)


def own_kernel(part, n_rep, gate, up, down, gate_up, down_own, d_same, d_other, g, u, d, sem):
    r = lax.axis_index("rep")
    pairs = [(gate, g), (up, u)]
    for m in range(n_rep):
        at = pl.ds(pl.multiple_of((r ^ m) * part, part), part)
        pairs.append((down.at[at], d.at[pl.ds(m * part, part)]))
    fetch(pairs, sem)
    half = gate.shape[1] // 2
    b = lax.axis_index("fs") & 1
    for case in range(2):

        @pl.when(b == case)
        def _():
            cut = slice(case * half, (case + 1) * half)
            gate_up[...] = jnp.concatenate([g[:, cut], u[:, cut]], axis=1)
            down_own[...] = d[:, cut]
            for ref, side in ((d_same, case), (d_other, 1 - case)):
                cut = slice(side * half, (side + 1) * half)
                ref[...] = jnp.concatenate([d[: part // 2, cut], d[part // 2 : part, cut]], axis=1)


def copy_kernel(x, out):
    out[...] = x[...]


def add_kernel(left, right, keep, send):
    total = (left[...].astype(f32) + right[...].astype(f32)).astype(bf16)
    cut = keep.shape[0]
    keep[...] = total[:cut]
    send[...] = total[cut:]


def rms_norm(x, gain):
    scale = lax.rsqrt(jnp.mean(x * x, axis=-1, keepdims=True) + epsilon)
    return (x * scale * gain).astype(bf16)


def mixer_kernel(cfg, tok_a, tok_b, gain, lgain, lshift, mkern, moff, fgain, *rest):
    bundles, (mid, normed2, wbuf, sem) = rest[: len(cfg["segments"])], rest[len(cfg["segments"]) :]
    k, r, t = lax.axis_index("fs"), lax.axis_index("rep"), lax.axis_index("tp")
    rows, part, lw, width = cfg["rows"], cfg["part"], cfg["lw"], cfg["width"]
    wide, n_tp, ny = cfg["wide"], cfg["n_tp"], cfg["n_tp"] // 2
    copies = []
    for ref, segs in zip(bundles, cfg["segments"]):
        for start, count, j, rr, tt in segs:
            base = (k ^ j) * rows
            if rr is not None:
                base = base + (r ^ rr) * part
            to = pl.ds(pl.multiple_of(base, part), count)
            for m in range(3):
                if wide:
                    place = wbuf.at[to, pl.ds(m * width + tt * lw, lw)]
                else:
                    place = wbuf.at[m * n_tp + tt, to]
                source = ref.at[m, pl.ds(start, count)]
                copies.append(pltpu.make_async_copy(source, place, sem.at[len(copies)]))
    for c in copies:
        c.start()
    h = tok_a.shape[0] // (2 * ny)
    span = mkern.shape[1]
    row = lax.broadcasted_iota(jnp.int32, (span, span), 0)
    col = lax.broadcasted_iota(jnp.int32, (span, span), 1)
    kerns, offsets = [], []
    for tt in range(n_tp):
        group = ((t ^ tt) * lw) // cfg["group_ch"]
        kerns.append(jnp.where(row >= col, mkern[group].astype(f32), 0.0).astype(bf16))
        offset = jnp.where(row == col, moff[group].astype(f32), 0.0)
        offsets.append(jnp.sum(offset, axis=1, keepdims=True))

    def block(i):
        yy, bb = i // 2, i % 2
        at_a, at_b = (yy * 2 + bb) * h, (bb * ny + yy) * h
        return [tok_a[at_a : at_a + h].astype(f32), tok_b[at_b : at_b + h].astype(f32)]

    def project(rows_in, m, tt):
        w = wbuf[:, m * width + tt * lw : m * width + (tt + 1) * lw] if wide else wbuf[m * n_tp + tt]
        return jnp.dot(rows_in, w, preferred_element_type=f32)

    waited = False
    for at in range(0, 2 * ny, 2):
        x = jnp.concatenate(block(at) + block(at + 1), axis=0)
        normed = rms_norm(x, gain[...].astype(f32))
        if not waited:
            for c in copies:
                c.wait()
            waited = True
        gate_u, act = [], []
        total = squares = 0.0
        if wide:
            pre = jnp.dot(normed, wbuf[:, : 2 * width], preferred_element_type=f32)
        for tt in range(n_tp):
            if wide:
                g = pre[:, tt * lw : (tt + 1) * lw]
                v = pre[:, width + tt * lw : width + (tt + 1) * lw]
            else:
                g, v = project(normed, 0, tt), project(normed, 1, tt)
            gate_u.append(jax.nn.gelu(g))
            a = jax.nn.gelu(v)
            act.append(a)
            total = total + jnp.sum(a, axis=-1, keepdims=True)
            squares = squares + jnp.sum(a * a, axis=-1, keepdims=True)
        center = total / width
        spread = squares / width - center * center
        inv = lax.rsqrt(spread + epsilon)
        gated, out = [], None
        for tt in range(n_tp):
            own = t ^ tt
            values = (
                (act[tt] - center) * inv * lgain[own].astype(f32) + lshift[own].astype(f32)
            ).astype(bf16)
            mixed = [
                jnp.dot(kerns[tt], values[i : i + span], preferred_element_type=f32) + offsets[tt]
                for i in range(0, values.shape[0], span)
            ]
            gated.append((gate_u[tt] * jnp.concatenate(mixed, axis=0)).astype(bf16))
            if not wide:
                term = contract_last(gated[tt], wbuf[2 * n_tp + tt])
                out = term if out is None else out + term
        if wide:
            out = contract_last(jnp.concatenate(gated, axis=1), wbuf[:, 2 * width :])
        middle = (x + out).astype(bf16)
        if at == 0:
            mid[...] = middle[: 2 * h]
        normed2[at * 2 * h : (at + 2) * 2 * h] = rms_norm(middle.astype(f32), fgain[...].astype(f32))


def hidden_kernel(cfg, *refs):
    final, blocks, where = cfg["final"], cfg["blocks"], cfg["where"]
    tokens, refs = refs[:2], refs[2:]
    if final:
        base, refs = refs[0], refs[1:]
    weights, (out, wbuf, sem) = refs[: len(where)], refs[len(where) :]
    rows, part = cfg["rows"], cfg["part"]
    k, r = lax.axis_index("fs"), lax.axis_index("rep")
    pairs = []
    for ref, (j, rr) in zip(weights, where):
        at = blocks.index(j) * rows
        if rr is not None:
            at = pl.multiple_of(at + (r ^ rr) * part, part)
        pairs.append((ref, wbuf.at[pl.ds(at, ref.shape[0])]))
    fetch(pairs, sem)
    half = out.shape[1] if final else out.shape[1] // 2
    start = 0
    for ref in tokens:
        for at in range(0, ref.shape[0], cfg["tile"]):
            here = pl.ds(start + at, cfg["tile"])
            pre = base[here] if final else None
            for i, j in enumerate(blocks):
                cols = pl.ds(pl.multiple_of((k ^ j) * rows, rows), rows)
                term = jnp.dot(
                    ref[pl.ds(at, cfg["tile"]), cols],
                    wbuf[i * rows : (i + 1) * rows],
                    preferred_element_type=f32,
                )
                pre = term if pre is None else pre + term
            if final:
                out[here] = (jax.nn.silu(pre[:, :half]) * pre[:, half:]).astype(bf16)
            else:
                out[here] = pre
        start += ref.shape[0]


def down_kernel(packed, hid, *refs):
    weights, (keep, send) = refs[:-2], refs[-2:]
    half = hid.shape[1]
    top = keep.shape[0]
    col = 0
    h = hid[...]
    for ref in weights:
        for i in range(2 if packed else 1):
            w = ref[:, i * half : (i + 1) * half]
            res = contract_last(h, w).astype(bf16)
            keep[:, col : col + w.shape[0]] = res[:top]
            send[:, col : col + w.shape[0]] = res[top:]
            col += w.shape[0]


def per_device(
    sizes,
    tokens,
    mix_gain,
    gate_proj,
    value_proj,
    layer_gain,
    layer_shift,
    mix_kernel,
    mix_offset,
    out_proj,
    ffn_gain,
    ffn_gate,
    ffn_up,
    ffn_down,
):
    n_rep, n_fs, n_tp = sizes
    r, k = lax.axis_index("rep"), lax.axis_index("fs")
    count, d_model = tokens.shape
    rows, lw = gate_proj.shape
    part = rows // n_rep
    width = layer_gain.shape[0]
    ff = ffn_gate.shape[1]
    half = ff // 2
    any_spec = pl.BlockSpec(memory_space=pl.ANY)
    hbm_spec = pl.BlockSpec(memory_space=pltpu.HBM)
    vmem_spec = pl.BlockSpec(memory_space=pltpu.VMEM)
    far_first = list(range(n_fs - 1, 0, -1))

    h = count // 2
    col_a, col_b = tokens[:h], tokens[h:]
    col_a = jnp.concatenate([col_a, xor_permute(col_a, "fs", 1, n_fs)], axis=0)
    for m in bits(n_tp, 2):
        col_a = jnp.concatenate([col_a, xor_permute(col_a, "tp", m, n_tp)], axis=0)
        col_b = jnp.concatenate([col_b, xor_permute(col_b, "tp", m, n_tp)], axis=0)
    col_b = jnp.concatenate([col_b, xor_permute(col_b, "fs", 1, n_fs)], axis=0)

    pack, mine = pl.pallas_call(
        functools.partial(pack_kernel, part),
        out_shape=[
            jax.ShapeDtypeStruct((3, rows, lw), bf16),
            jax.ShapeDtypeStruct((3, part, lw), bf16),
        ],
        in_specs=[hbm_spec] * 3,
        out_specs=[vmem_spec] * 2,
        scratch_shapes=[pltpu.SemaphoreType.DMA((6,))],
        compiler_params=pltpu.CompilerParams(vmem_limit_bytes=4 * MIB),
        name="pack",
    )(gate_proj, value_proj, out_proj)
    got = {j: xor_permute(mine, "fs", j, n_fs) for j in far_first}

    gu_same, gu_other = pl.pallas_call(
        functools.partial(send_kernel, part),
        out_shape=[jax.ShapeDtypeStruct((part, ff), bf16)] * 2,
        in_specs=[any_spec] * 2,
        out_specs=[vmem_spec] * 2,
        scratch_shapes=[pltpu.VMEM((part, ff), bf16)] * 2 + [pltpu.SemaphoreType.DMA((2,))],
        compiler_params=pltpu.CompilerParams(vmem_limit_bytes=8 * MIB),
        cost_estimate=pl.CostEstimate(flops=0, bytes_accessed=8 * part * ff, transcendentals=0),
        name="prepsend",
    )(ffn_gate, ffn_up)
    gu_z = {j: xor_permute(gu_other if j & 1 else gu_same, "fs", j, n_fs) for j in far_first}
    gu_weights, gu_where = [None], [(0, None)]
    for j in far_first:
        gu_weights.append(gu_z[j])
        gu_where.append((j, 0))
        for m in range(1, n_rep):
            gu_weights.append(xor_permute(gu_z[j], "rep", m, n_rep))
            gu_where.append((j, m))

    gate_up, down_own, d_same, d_other = pl.pallas_call(
        functools.partial(own_kernel, part, n_rep),
        out_shape=[
            jax.ShapeDtypeStruct((rows, ff), bf16),
            jax.ShapeDtypeStruct((rows, half), bf16),
            jax.ShapeDtypeStruct((part // 2, ff), bf16),
            jax.ShapeDtypeStruct((part // 2, ff), bf16),
        ],
        in_specs=[any_spec] * 3,
        out_specs=[vmem_spec] * 4,
        scratch_shapes=[pltpu.VMEM((rows, ff), bf16)] * 3
        + [pltpu.SemaphoreType.DMA((2 + n_rep,))],
        compiler_params=pltpu.CompilerParams(vmem_limit_bytes=16 * MIB),
        cost_estimate=pl.CostEstimate(flops=0, bytes_accessed=12 * rows * ff, transcendentals=0),
        name="prepown",
    )(ffn_gate, ffn_up, ffn_down)

    def exchange(bundles, axis, m, n):
        arrays, segs, at = [], [], 0
        for array, entries in bundles:
            if axis == "rep":
                entries = [e for e in entries if e[3] is not None]
                if not entries:
                    continue
            arrays.append(array)
            for start, num, j, rr, tt in entries:
                if axis == "rep":
                    rr = rr ^ m
                else:
                    tt = tt ^ m
                segs.append((start + at, num, j, rr, tt))
            at += array.shape[1]
        joined = arrays[0] if len(arrays) == 1 else jnp.concatenate(arrays, axis=1)
        return (xor_permute(joined, axis, m, n), segs)

    smalls = (
        mix_gain[None],
        layer_gain.reshape(n_tp, 1, lw),
        layer_shift.reshape(n_tp, 1, lw),
        mix_offset[:, None, :],
        ffn_gain[None],
    )
    got[1], smalls = lax.optimization_barrier((got[1], smalls))
    gain = pl.pallas_call(
        copy_kernel,
        out_shape=jax.ShapeDtypeStruct(smalls[0].shape, bf16),
        in_specs=[vmem_spec],
        out_specs=vmem_spec,
        compiler_params=pltpu.CompilerParams(vmem_limit_bytes=1 * MIB),
        cost_estimate=pl.CostEstimate(flops=2048, bytes_accessed=8192, transcendentals=0),
        name="mark",
    )(smalls[0])
    smalls = (gain,) + smalls[1:]

    near = [(pack, [(0, rows, 0, None, 0)])]
    near += [(got[j], [(0, part, j, 0, 0)]) for j in range(1, n_fs // 2)]
    far = [(got[j], [(0, part, j, 0, 0)]) for j in range(n_fs // 2, n_fs)]
    steps = [("rep", m, n_rep) for m in bits(n_rep)] + [("tp", m, n_tp) for m in bits(n_tp, 2)]
    for step in steps:
        near.append(exchange(near, *step))
    for step in reversed(steps):
        far.append(exchange(far, *step))
    bundles = near + far
    for bundle in list(bundles):
        bundles.append(exchange([bundle], "tp", 1, n_tp))

    gu_weights[0] = gate_up
    segments = [segs for _, segs in bundles]
    cfg = dict(
        rows=rows,
        part=part,
        lw=lw,
        width=width,
        group_ch=width // mix_kernel.shape[0],
        segments=segments,
    )
    n_copies = 3 * sum(len(s) for s in segments)
    wide = lw % 128 == 0
    core_tokens = col_a.shape[0] + col_b.shape[0]
    cfg.update(wide=wide, n_tp=n_tp)
    middle, normed2 = pl.pallas_call(
        functools.partial(mixer_kernel, cfg),
        out_shape=[
            jax.ShapeDtypeStruct((count, d_model), bf16),
            jax.ShapeDtypeStruct((core_tokens, d_model), bf16),
        ],
        in_specs=[vmem_spec] * 8 + [any_spec] * len(bundles),
        out_specs=[vmem_spec] * 2,
        scratch_shapes=[
            pltpu.VMEM((d_model, 3 * width) if wide else (3 * n_tp, d_model, lw), bf16),
            pltpu.SemaphoreType.DMA((n_copies,)),
        ],
        compiler_params=pltpu.CompilerParams(vmem_limit_bytes=32 * MIB),
        cost_estimate=pl.CostEstimate(
            flops=6 * core_tokens * d_model * width,
            bytes_accessed=6 * d_model * width,
            transcendentals=2 * core_tokens * width,
        ),
        name="mixer",
    )(
        col_a,
        col_b,
        *smalls[:3],
        mix_kernel,
        *smalls[3:],
        *[array for array, _ in bundles],
    )

    groups = [normed2, xor_permute(normed2, "tp", 1, n_tp)]
    group_tokens = sum(g.shape[0] for g in groups)

    d_z = {j: xor_permute(d_other if j & 1 else d_same, "fs", j, n_fs) for j in far_first}
    d_x = {j: [xor_permute(d_z[j], "rep", m, n_rep) for m in range(1, n_rep)] for j in far_first}

    last = n_fs // 2

    def hidden_call(final, blocks, extra):
        chosen = [(w, p) for w, p in zip(gu_weights, gu_where) if p[0] in blocks]
        width_out, kind = (half, bf16) if final else (ff, f32)
        return pl.pallas_call(
            functools.partial(
                hidden_kernel,
                dict(
                    rows=rows,
                    part=part,
                    final=final,
                    blocks=blocks,
                    where=[p for _, p in chosen],
                    tile=min(256, core_tokens),
                ),
            ),
            out_shape=jax.ShapeDtypeStruct((group_tokens, width_out), kind),
            in_specs=[vmem_spec] * (2 + len(extra)) + [any_spec] * len(chosen),
            out_specs=vmem_spec,
            scratch_shapes=[
                pltpu.VMEM((rows * len(blocks), ff), bf16),
                pltpu.SemaphoreType.DMA((len(chosen),)),
            ],
            compiler_params=pltpu.CompilerParams(vmem_limit_bytes=24 * MIB),
            cost_estimate=pl.CostEstimate(
                flops=2 * group_tokens * rows * len(blocks) * ff,
                bytes_accessed=2 * d_model * group_tokens,
                transcendentals=group_tokens * half,
            ),
        )(*groups, *extra, *[w for w, _ in chosen])

    first_blocks = [j for j in range(n_fs) if j != last]
    begun = hidden_call(False, first_blocks, [])
    hidden = hidden_call(True, [last], [begun])

    def down(weights, packed):
        return pl.pallas_call(
            functools.partial(down_kernel, packed),
            out_shape=[jax.ShapeDtypeStruct((group_tokens // 2, rows), bf16)] * 2,
            in_specs=[vmem_spec] * (1 + len(weights)),
            out_specs=[vmem_spec] * 2,
            compiler_params=pltpu.CompilerParams(vmem_limit_bytes=12 * MIB),
            cost_estimate=pl.CostEstimate(
                flops=2 * group_tokens * half * rows,
                bytes_accessed=2 * group_tokens * (half + rows),
                transcendentals=0,
            ),
        )(hidden, *weights)

    def add(left, right):
        cut = left.shape[0] // 2
        return pl.pallas_call(
            add_kernel,
            out_shape=[jax.ShapeDtypeStruct((cut, left.shape[1]), bf16)] * 2,
            in_specs=[vmem_spec] * 2,
            out_specs=[vmem_spec] * 2,
            compiler_params=pltpu.CompilerParams(vmem_limit_bytes=6 * MIB),
            cost_estimate=pl.CostEstimate(
                flops=left.size, bytes_accessed=8 * left.size, transcendentals=0
            ),
        )(left, right)

    kept, sent = {}, {}
    for j in range(n_fs):
        keep, send = down([d_z[j]] + d_x[j] if j else [down_own], j > 0)
        keep, send = add(keep, xor_permute(send, "tp", 1, n_tp))
        for m in reversed(bits(n_tp, 2)):
            keep, send = add(keep, xor_permute(send, "tp", m, n_tp))
        kept[j] = keep
        sent[j] = xor_permute(send, "fs", 1, n_fs)
    pieces = []
    for j in range(n_fs):
        total = kept[j].astype(f32) + sent[j ^ 1].astype(f32)
        pieces.append(
            jnp.concatenate(
                absolute([total[:, m * part : (m + 1) * part] for m in range(n_rep)], r), axis=1
            )
        )
    summed = jnp.concatenate(absolute(pieces, k), axis=1)
    return (middle.astype(f32) + summed).astype(bf16)


def solution(mesh):
    token_spec = P(("rep", "fs", "tp"), None)
    weight_spec = P("fs", "tp")
    placed = (
        token_spec,
        P(),
        weight_spec,
        weight_spec,
        P(),
        P(),
        P(),
        P(),
        weight_spec,
        P(),
        weight_spec,
        weight_spec,
        weight_spec,
    )
    sizes = (mesh.shape["rep"], mesh.shape["fs"], mesh.shape["tp"])

    def body(*args):
        return per_device(sizes, *args)

    return jax.shard_map(
        body, mesh=mesh, in_specs=placed, out_specs=token_spec, check_vma=False
    )
```

time: 258 us -> 245 us (0.950)
  other arithmetic: 9.3 us -> 1.62 us
  waiting for transfers between devices: 161 us -> 156 us
  Pallas kernels: 24 us -> 27.7 us
    ppermute x45 -> x44, waiting for transfers between devices: 161 us -> 156 us  [xor_permute(): return lax.ppermute(x, axis, [(i, i ^ m) for i in range(n)])]
    pallas_call x1 -> x13, Pallas kernels: 9.07 us -> 12.5 us  [the longest x2 9.13 us: hidden_call(): pl.pallas_call(functools.partial(hidden_kernel, dict(rows=rows, part=part...]
    select_n x3 -> x0, other arithmetic: 3.41 us -> none  [columns(): return jnp.where(which == 0, w[:, :half], w[:, half:])]
    convert_element_type x12 -> x0, other arithmetic: 2.9 us -> none  [add(): return (left.astype(f32) + right.astype(f32)).astype(bf16)]
    unnamed x32 -> x22, local copies, waits for them, and re-layouts: 5.45 us -> 2.76 us
    ppermute x45 -> x44, starting transfers between devices: 55.4 us -> 54.8 us  [xor_permute(): return lax.ppermute(x, axis, [(i, i ^ m) for i in range(n)])]
  transfers between devices with their start and end apart: 45 -> 44, of which waited for: 21 -> 21; matrix products, arithmetic and copies ran while one was open for 3% -> 1% of each run, Pallas kernels for 7% -> 8%
where the time goes in v1:
time: 245 us
  waiting for transfers between devices  156 us (64%)
  starting transfers between devices  54.8 us (22%)
  Pallas kernels  27.7 us (11%)
  local copies, waits for them, and re-layouts  4.19 us (2%)
    ppermute x44, waiting for transfers between devices, xor_permute(): return lax.ppermute(x, axis, [(i, i ^ m) for i in range(n)])  156 us
    ppermute x44, starting transfers between devices, xor_permute(): return lax.ppermute(x, axis, [(i, i ^ m) for i in range(n)])  54.8 us
    pallas_call x2, Pallas kernels, hidden_call(): pl.pallas_call(functools.partial(hidden_kernel, dict(rows=rows, part=part...  9.13 us
    pallas_call x1, Pallas kernels, per_device(): pl.pallas_call(functools.partial(mixer_kernel, cfg), out_shape=[jax.Shape...  7.89 us
    pallas_call x4, Pallas kernels, down(): pl.pallas_call(functools.partial(down_kernel, packed), out_shape=[jax.Sha...  6.54 us
  transfers between devices with their start and end apart: 44, of which 21 were waited for; matrix products, arithmetic and copies ran while one was open for 1% of the time, Pallas kernels for 8%

profile of v1, /device:TPU:0, one launch (start us, length us, event | category | flops | bytes accessed | tf_op | source)
XLA Modules:
  0.0 244.8 jit_solution(12296691335841904595)
XLA Ops:
  3.5 4.1 %collective-permute-start.7 = (bf16[3,256,128]{2,1,0:T(8,128)(2,1)S(1)}, bf16[3,256,128]{2,1,0:T(8,128)(2,1)S(1)}, u32[]{:S(2)}, u32[]{:S(2)}) collective-permute-start(bf16[3,256,128]{2,1,0:T(8,128)(2,1)S(1)} %get-tuple-element.45), channel_id=1, source_target_pairs={{0,8},{4,12},{8,0},{12,4},{1,9},{5,13},{9,1},{13,5},{2,10},{6,14},... | collective-permute-start | bytes 589832 | tf_op jit(solution)/shard_map/ppermute | solution.py:17
  9.2 12.6 %collective-permute-done.7.rest_4_ = bf16[3,256,128]{2,1,0:T(8,128)(2,1)S(1)} collective-permute-done((bf16[3,256,128]{2,1,0:T(8,128)(2,1)S(1)}, bf16[3,256,128]{2,1,0:T(8,128)(2,1)S(1)}, u32[]{:S(2)}, u32[]{:S(2)}) %collective-permute-start.7) | collective-permute-done | bytes 196640 | tf_op jit(solution)/shard_map/ppermute | solution.py:17
  21.9 1.9 collective-permute-start.9
  26.7 4.2 %collective-permute-done.5.rest_2_ = bf16[3,256,128]{2,1,0:T(8,128)(2,1)S(1)} collective-permute-done((bf16[3,256,128]{2,1,0:T(8,128)(2,1)S(1)}, bf16[3,256,128]{2,1,0:T(8,128)(2,1)S(1)}, u32[]{:S(2)}, u32[]{:S(2)}) %collective-permute-start.5) | collective-permute-done | bytes 196640 | tf_op jit(solution)/shard_map/ppermute | solution.py:17
  33.7 2.5 %collective-permute-start.2 = (bf16[64,2048]{1,0:T(8,128)(2,1)S(1)}, bf16[64,2048]{1,0:T(8,128)(2,1)S(1)}, u32[]{:S(2)}, u32[]{:S(2)}) collective-permute-start(bf16[64,2048]{1,0:T(8,128)(2,1)S(1)} %get-tuple-element.89), channel_id=1, source_target_pairs={{0,2},{1,3},{2,0},{3,1},{4,6},{5,7},{6,4},{7,5},{8,10},{9,11},{10,... | collective-permute-start | bytes 786440 | tf_op jit(solution)/shard_map/ppermute | solution.py:17
  36.3 5.0 %collective-permute-start = (bf16[64,2048]{1,0:T(8,128)(2,1)S(1)}, bf16[64,2048]{1,0:T(8,128)(2,1)S(1)}, u32[]{:S(2)}, u32[]{:S(2)}) collective-permute-start(bf16[64,2048]{1,0:T(8,128)(2,1)S(1)} %get-tuple-element.90), channel_id=1, source_target_pairs={{0,4},{4,0},{8,12},{12,8},{1,5},{5,1},{9,13},{13,9},{2,6},{6,2},{1... | collective-permute-start | bytes 786440 | tf_op jit(solution)/shard_map/ppermute | solution.py:17
  41.3 12.6 %collective-permute-done.2 = bf16[64,2048]{1,0:T(8,128)(2,1)S(1)} collective-permute-done((bf16[64,2048]{1,0:T(8,128)(2,1)S(1)}, bf16[64,2048]{1,0:T(8,128)(2,1)S(1)}, u32[]{:S(2)}, u32[]{:S(2)}) %collective-permute-start.2) | collective-permute-done | bytes 262176 | tf_op jit(solution)/shard_map/ppermute | solution.py:17
  53.9 5.8 %collective-permute-start.3 = (bf16[128,2048]{1,0:T(8,128)(2,1)S(1)}, bf16[128,2048]{1,0:T(8,128)(2,1)S(1)}, u32[]{:S(2)}, u32[]{:S(2)}) collective-permute-start(bf16[128,2048]{1,0:T(8,128)(2,1)S(1)} %pad_maximum_fusion.5), channel_id=1, source_target_pairs={{0,4},{4,0},{8,12},{12,8},{1,5},{5,1},{9,13},{13,9},{2,6},{6,2},{1... | collective-permute-start | bytes 1572872 | tf_op jit(solution)/shard_map/ppermute | solution.py:17
  64.2 5.6 %collective-permute-done.3 = bf16[128,2048]{1,0:T(8,128)(2,1)S(1)} collective-permute-done((bf16[128,2048]{1,0:T(8,128)(2,1)S(1)}, bf16[128,2048]{1,0:T(8,128)(2,1)S(1)}, u32[]{:S(2)}, u32[]{:S(2)}) %collective-permute-start.3) | collective-permute-done | bytes 524320 | tf_op jit(solution)/shard_map/ppermute | solution.py:17
  70.0 5.2 %collective-permute-done.1 = bf16[128,2048]{1,0:T(8,128)(2,1)S(1)} collective-permute-done((bf16[128,2048]{1,0:T(8,128)(2,1)S(1)}, bf16[128,2048]{1,0:T(8,128)(2,1)S(1)}, u32[]{:S(2)}, u32[]{:S(2)}) %collective-permute-start.1) | collective-permute-done | bytes 524320 | tf_op jit(solution)/shard_map/ppermute | solution.py:17
  76.6 7.9 %mixer.1 = (bf16[128,2048]{1,0:T(8,128)(2,1)S(1)}, bf16[512,2048]{1,0:T(8,128)(2,1)S(1)}) custom-call(bf16[256,2048]{1,0:T(8,128)(2,1)S(1)} %pad_maximum_fusion.tok_a, bf16[256,2048]{1,0:T(8,128)(2,1)S(1)} %pad_maximum_fusion.1.tok_b, bf16[1,2048]{1,0:T(2,128)(2,1)S(1)} %mark.1.gain, bf16[4,1,128]{2,1,0:T(2,128)(2,1)S(1)} %copy.14.lgain, ...), custom_call_target="tpu_custom_call" | custom-call | flops 3221225472 | bytes 6291456 | tf_op jit(solution)/shard_map/mixer/pallas_call | solution.py:404
  85.6 3.5 %collective-permute-start.20 = (bf16[256,1408]{1,0:T(8,128)(2,1)S(1)}, bf16[256,1408]{1,0:T(8,128)(2,1)S(1)}, u32[]{:S(2)}, u32[]{:S(2)}) collective-permute-start(bf16[256,1408]{1,0:T(8,128)(2,1)S(1)} %get-tuple-element.56), channel_id=1, source_target_pairs={{0,12},{4,8},{8,4},{12,0},{1,13},{5,9},{9,5},{13,1},{2,14},{6,10},... | collective-permute-start | bytes 2162696 | tf_op jit(solution)/shard_map/ppermute | solution.py:17
  90.8 2.3 collective-permute-start.36
  93.1 45.5 %collective-permute-done.36.refs_0_ = bf16[128,1408]{1,0:T(8,128)(2,1)S(1)} collective-permute-done((bf16[128,1408]{1,0:T(8,128)(2,1)S(1)}, bf16[128,1408]{1,0:T(8,128)(2,1)S(1)}, u32[]{:S(2)}, u32[]{:S(2)}) %collective-permute-start.36) | collective-permute-done | bytes 360480 | tf_op jit(solution)/shard_map/ppermute | solution.py:17
  141.1 25.1 %collective-permute-done.30.refs_0_ = bf16[128,1408]{1,0:T(8,128)(2,1)S(1)} collective-permute-done((bf16[128,1408]{1,0:T(8,128)(2,1)S(1)}, bf16[128,1408]{1,0:T(8,128)(2,1)S(1)}, u32[]{:S(2)}, u32[]{:S(2)}) %collective-permute-start.30) | collective-permute-done | bytes 360480 | tf_op jit(solution)/shard_map/ppermute | solution.py:17
  166.2 2.6 %collective-permute-start.26 = (bf16[128,1408]{1,0:T(8,128)(2,1)S(1)}, bf16[128,1408]{1,0:T(8,128)(2,1)S(1)}, u32[]{:S(2)}, u32[]{:S(2)}) collective-permute-start(bf16[128,1408]{1,0:T(8,128)(2,1)S(1)} %get-tuple-element.58), channel_id=1, source_target_pairs={{0,12},{4,8},{8,4},{12,0},{1,13},{5,9},{9,5},{13,1},{2,14},{6,10},... | collective-permute-start | bytes 1081352 | tf_op jit(solution)/shard_map/ppermute | solution.py:17
  170.3 7.9 %collective-permute-done.26.refs_0_ = bf16[128,1408]{1,0:T(8,128)(2,1)S(1)} collective-permute-done((bf16[128,1408]{1,0:T(8,128)(2,1)S(1)}, bf16[128,1408]{1,0:T(8,128)(2,1)S(1)}, u32[]{:S(2)}, u32[]{:S(2)}) %collective-permute-start.26) | collective-permute-done | bytes 360480 | tf_op jit(solution)/shard_map/ppermute | solution.py:17
  181.7 6.6 %shard_map.127.refs_2_ = f32[1024,1408]{1,0:T(8,128)S(1)} custom-call(bf16[512,2048]{1,0:T(8,128)(2,1)S(1)} %get-tuple-element.54.refs_0_, bf16[512,2048]{1,0:T(8,128)(2,1)S(1)} %collective-permute-done.19.refs_1_, bf16[512,1408]{1,0:T(8,128)(2,1)S(1)} %get-tuple-element.55.refs_2_, bf16[256,1408]{1,0:T(8,128)(2,1)S(1)} %collective-permute-done.20.refs_3_, ...), custom_call_target="tpu_custom_call" | custom-call | flops 4429185024 | bytes 4194304 | tf_op jit(solution)/shard_map/pallas_call | solution.py:443
  188.9 2.6 %shard_map.128.hid = bf16[1024,704]{1,0:T(8,128)(2,1)S(1)} custom-call(bf16[512,2048]{1,0:T(8,128)(2,1)S(1)} %get-tuple-element.54.refs_0_, bf16[512,2048]{1,0:T(8,128)(2,1)S(1)} %collective-permute-done.19.refs_1_, f32[1024,1408]{1,0:T(8,128)S(1)} %shard_map.127.refs_2_, bf16[256,1408]{1,0:T(8,128)(2,1)S(1)} %collective-permute-done.24.refs_3_, ...), custom_call_target="tpu_custom_call" | custom-call | flops 1476395008 | bytes 4194304 | tf_op jit(solution)/shard_map/pallas_call | solution.py:443
  192.6 4.1 %collective-permute-done.37.refs_1_ = bf16[128,1408]{1,0:T(8,128)(2,1)S(1)} collective-permute-done((bf16[128,1408]{1,0:T(8,128)(2,1)S(1)}, bf16[128,1408]{1,0:T(8,128)(2,1)S(1)}, u32[]{:S(2)}, u32[]{:S(2)}) %collective-permute-start.37) | collective-permute-done | bytes 360480 | tf_op jit(solution)/shard_map/ppermute | solution.py:17
  196.7 1.8 shard_map.135
  198.6 5.8 %collective-permute-done.31.refs_1_ = bf16[128,1408]{1,0:T(8,128)(2,1)S(1)} collective-permute-done((bf16[128,1408]{1,0:T(8,128)(2,1)S(1)}, bf16[128,1408]{1,0:T(8,128)(2,1)S(1)}, u32[]{:S(2)}, u32[]{:S(2)}) %collective-permute-start.31) | collective-permute-done | bytes 360480 | tf_op jit(solution)/shard_map/ppermute | solution.py:17
  206.3 4.4 %collective-permute-done.27.refs_1_ = bf16[128,1408]{1,0:T(8,128)(2,1)S(1)} collective-permute-done((bf16[128,1408]{1,0:T(8,128)(2,1)S(1)}, bf16[128,1408]{1,0:T(8,128)(2,1)S(1)}, u32[]{:S(2)}, u32[]{:S(2)}) %collective-permute-start.27) | collective-permute-done | bytes 360480 | tf_op jit(solution)/shard_map/ppermute | solution.py:17
  217.5 4.5 %collective-permute-done.41.right = bf16[256,512]{1,0:T(8,128)(2,1)S(1)} collective-permute-done((bf16[256,512]{1,0:T(8,128)(2,1)S(1)}, bf16[256,512]{1,0:T(8,128)(2,1)S(1)}, u32[]{:S(2)}, u32[]{:S(2)}) %collective-permute-start.41) | collective-permute-done | bytes 262176 | tf_op jit(solution)/shard_map/ppermute | solution.py:17
  222.1 1.9 collective-permute-start.42
  224.0 3.7 %collective-permute-done.39.right = bf16[256,512]{1,0:T(8,128)(2,1)S(1)} collective-permute-done((bf16[256,512]{1,0:T(8,128)(2,1)S(1)}, bf16[256,512]{1,0:T(8,128)(2,1)S(1)}, u32[]{:S(2)}, u32[]{:S(2)}) %collective-permute-start.39) | collective-permute-done | bytes 262176 | tf_op jit(solution)/shard_map/ppermute | solution.py:17
  227.7 1.9 collective-permute-start.43
  229.6 3.7 %collective-permute-done.33.right = bf16[256,512]{1,0:T(8,128)(2,1)S(1)} collective-permute-done((bf16[256,512]{1,0:T(8,128)(2,1)S(1)}, bf16[256,512]{1,0:T(8,128)(2,1)S(1)}, u32[]{:S(2)}, u32[]{:S(2)}) %collective-permute-start.33) | collective-permute-done | bytes 262176 | tf_op jit(solution)/shard_map/ppermute | solution.py:17
  233.4 1.9 collective-permute-start.34
  235.3 3.2 %collective-permute-done.29.right = bf16[256,512]{1,0:T(8,128)(2,1)S(1)} collective-permute-done((bf16[256,512]{1,0:T(8,128)(2,1)S(1)}, bf16[256,512]{1,0:T(8,128)(2,1)S(1)}, u32[]{:S(2)}, u32[]{:S(2)}) %collective-permute-start.29) | collective-permute-done | bytes 262176 | tf_op jit(solution)/shard_map/ppermute | solution.py:17
  238.5 1.9 collective-permute-start.35
  240.6 3.1 %collective-permute-done.35 = bf16[128,512]{1,0:T(8,128)(2,1)S(1)} collective-permute-done((bf16[128,512]{1,0:T(8,128)(2,1)S(1)}, bf16[128,512]{1,0:T(8,128)(2,1)S(1)}, u32[]{:S(2)}, u32[]{:S(2)}) %collective-permute-start.35) | collective-permute-done | bytes 131104 | tf_op jit(solution)/shard_map/ppermute | solution.py:17
  (121 shorter events, 39.0 us)
Async XLA Ops:
  3.5 18.4 %collective-permute-start.7 = (bf16[3,256,128]{2,1,0:T(8,128)(2,1)S(1)}, bf16[3,256,128]{2,1,0:T(8,128)(2,1)S(1)}, u32[]{:S(2)}, u32[]{:S(2)}) collective-permute-start(bf16[3,256,128]{2,1,0:T(8,128)(2,1)S(1)} %get-tuple-element.45), channel_id=1, source_target_pairs={{0,8},{4,12},{8,0},{12,4},{1,9},{5,13},{9,1},{13,5},{2,10},{6,14},... | collective-permute-start | bytes 589832 | tf_op jit(solution)/shard_map/ppermute | solution.py:17
  7.6 14.2 %collective-permute-start.8 = (bf16[3,256,128]{2,1,0:T(8,128)(2,1)S(1)}, bf16[3,256,128]{2,1,0:T(8,128)(2,1)S(1)}, u32[]{:S(2)}, u32[]{:S(2)}) collective-permute-start(bf16[3,256,128]{2,1,0:T(8,128)(2,1)S(1)} %get-tuple-element.45), channel_id=1, source_target_pairs={{0,12},{4,8},{8,4},{12,0},{1,13},{5,9},{9,5},{13,1},{2,14},{6,10},... | collective-permute-start | bytes 589832 | tf_op jit(solution)/shard_map/ppermute | solution.py:17
  9.0 16.2 %collective-permute-start.4 = (bf16[3,256,128]{2,1,0:T(8,128)(2,1)S(1)}, bf16[3,256,128]{2,1,0:T(8,128)(2,1)S(1)}, u32[]{:S(2)}, u32[]{:S(2)}) collective-permute-start(bf16[3,256,128]{2,1,0:T(8,128)(2,1)S(1)} %get-tuple-element.45), channel_id=1, source_target_pairs={{0,4},{4,0},{8,12},{12,8},{1,5},{5,1},{9,13},{13,9},{2,6},{6,2},{1... | collective-permute-start | bytes 589832 | tf_op jit(solution)/shard_map/ppermute | solution.py:17
  31.0 29.3 %collective-permute-start.6 = (bf16[3,1024,128]{2,1,0:T(8,128)(2,1)S(1)}, bf16[3,1024,128]{2,1,0:T(8,128)(2,1)S(1)}, u32[]{:S(2)}, u32[]{:S(2)}) collective-permute-start(bf16[3,1024,128]{2,1,0:T(8,128)(2,1)S(1)} %pad_maximum_fusion.2), channel_id=1, source_target_pairs={{0,2},{1,3},{2,0},{3,1},{4,6},{5,7},{6,4},{7,5},{8,10},{9,11},{10,... | collective-permute-start | bytes 2359304 | tf_op jit(solution)/shard_map/ppermute | solution.py:17
  32.5 27.9 %collective-permute-start.10 = (bf16[3,1024,128]{2,1,0:T(8,128)(2,1)S(1)}, bf16[3,1024,128]{2,1,0:T(8,128)(2,1)S(1)}, u32[]{:S(2)}, u32[]{:S(2)}) collective-permute-start(bf16[3,1024,128]{2,1,0:T(8,128)(2,1)S(1)} %pad_maximum_fusion.3), channel_id=1, source_target_pairs={{0,16},{16,0},{1,17},{17,1},{2,18},{18,2},{3,19},{19,3},{4,20},{20... | collective-permute-start | bytes 2359304 | tf_op jit(solution)/shard_map/ppermute | solution.py:17
  33.7 20.1 %collective-permute-start.2 = (bf16[64,2048]{1,0:T(8,128)(2,1)S(1)}, bf16[64,2048]{1,0:T(8,128)(2,1)S(1)}, u32[]{:S(2)}, u32[]{:S(2)}) collective-permute-start(bf16[64,2048]{1,0:T(8,128)(2,1)S(1)} %get-tuple-element.89), channel_id=1, source_target_pairs={{0,2},{1,3},{2,0},{3,1},{4,6},{5,7},{6,4},{7,5},{8,10},{9,11},{10,... | collective-permute-start | bytes 786440 | tf_op jit(solution)/shard_map/ppermute | solution.py:17
  36.3 23.5 %collective-permute-start = (bf16[64,2048]{1,0:T(8,128)(2,1)S(1)}, bf16[64,2048]{1,0:T(8,128)(2,1)S(1)}, u32[]{:S(2)}, u32[]{:S(2)}) collective-permute-start(bf16[64,2048]{1,0:T(8,128)(2,1)S(1)} %get-tuple-element.90), channel_id=1, source_target_pairs={{0,4},{4,0},{8,12},{12,8},{1,5},{5,1},{9,13},{13,9},{2,6},{6,2},{1... | collective-permute-start | bytes 786440 | tf_op jit(solution)/shard_map/ppermute | solution.py:17
  53.9 16.0 %collective-permute-start.3 = (bf16[128,2048]{1,0:T(8,128)(2,1)S(1)}, bf16[128,2048]{1,0:T(8,128)(2,1)S(1)}, u32[]{:S(2)}, u32[]{:S(2)}) collective-permute-start(bf16[128,2048]{1,0:T(8,128)(2,1)S(1)} %pad_maximum_fusion.5), channel_id=1, source_target_pairs={{0,4},{4,0},{8,12},{12,8},{1,5},{5,1},{9,13},{13,9},{2,6},{6,2},{1... | collective-permute-start | bytes 1572872 | tf_op jit(solution)/shard_map/ppermute | solution.py:17
  60.3 16.3 %collective-permute-start.14 = (bf16[3,1024,128]{2,1,0:T(8,128)(2,1)S(1)}, bf16[3,1024,128]{2,1,0:T(8,128)(2,1)S(1)}, u32[]{:S(2)}, u32[]{:S(2)}) collective-permute-start(bf16[3,1024,128]{2,1,0:T(8,128)(2,1)S(1)} %collective-permute-done.6.rest_3_), channel_id=1, source_target_pairs={{0,1},{1,0},{2,3},{3,2},{4,5},{5,4},{6,7},{7,6},{8,9},{9,8},{10,11... | collective-permute-start | bytes 2359304 | tf_op jit(solution)/shard_map/ppermute | solution.py:17
  60.3 16.3 %collective-permute-start.18 = (bf16[3,1024,128]{2,1,0:T(8,128)(2,1)S(1)}, bf16[3,1024,128]{2,1,0:T(8,128)(2,1)S(1)}, u32[]{:S(2)}, u32[]{:S(2)}) collective-permute-start(bf16[3,1024,128]{2,1,0:T(8,128)(2,1)S(1)} %collective-permute-done.10.rest_7_), channel_id=1, source_target_pairs={{0,1},{1,0},{2,3},{3,2},{4,5},{5,4},{6,7},{7,6},{8,9},{9,8},{10,11... | collective-permute-start | bytes 2359304 | tf_op jit(solution)/shard_map/ppermute | solution.py:17
  61.2 14.0 %collective-permute-start.1 = (bf16[128,2048]{1,0:T(8,128)(2,1)S(1)}, bf16[128,2048]{1,0:T(8,128)(2,1)S(1)}, u32[]{:S(2)}, u32[]{:S(2)}) collective-permute-start(bf16[128,2048]{1,0:T(8,128)(2,1)S(1)} %pad_maximum_fusion.4), channel_id=1, source_target_pairs={{0,2},{1,3},{2,0},{3,1},{4,6},{5,7},{6,4},{7,5},{8,10},{9,11},{10,... | collective-permute-start | bytes 1572872 | tf_op jit(solution)/shard_map/ppermute | solution.py:17
  64.1 11.2 %collective-permute-start.11 = (bf16[3,512,128]{2,1,0:T(8,128)(2,1)S(1)}, bf16[3,512,128]{2,1,0:T(8,128)(2,1)S(1)}, u32[]{:S(2)}, u32[]{:S(2)}) collective-permute-start(bf16[3,512,128]{2,1,0:T(8,128)(2,1)S(1)} %get-tuple-element.51.rest_0_), channel_id=1, source_target_pairs={{0,1},{1,0},{2,3},{3,2},{4,5},{5,4},{6,7},{7,6},{8,9},{9,8},{10,11... | collective-permute-start | bytes 1179656 | tf_op jit(solution)/shard_map/ppermute | solution.py:17
  84.5 97.2 %collective-permute-start.19 = (bf16[512,2048]{1,0:T(8,128)(2,1)S(1)}, bf16[512,2048]{1,0:T(8,128)(2,1)S(1)}, u32[]{:S(2)}, u32[]{:S(2)}) collective-permute-start(bf16[512,2048]{1,0:T(8,128)(2,1)S(1)} %get-tuple-element.54.refs_0_), channel_id=1, source_target_pairs={{0,1},{1,0},{2,3},{3,2},{4,5},{5,4},{6,7},{7,6},{8,9},{9,8},{10,11... | collective-permute-start | bytes 6291464 | tf_op jit(solution)/shard_map/ppermute | solution.py:17
  85.6 53.4 %collective-permute-start.20 = (bf16[256,1408]{1,0:T(8,128)(2,1)S(1)}, bf16[256,1408]{1,0:T(8,128)(2,1)S(1)}, u32[]{:S(2)}, u32[]{:S(2)}) collective-permute-start(bf16[256,1408]{1,0:T(8,128)(2,1)S(1)} %get-tuple-element.56), channel_id=1, source_target_pairs={{0,12},{4,8},{8,4},{12,0},{1,13},{5,9},{9,5},{13,1},{2,14},{6,10},... | collective-permute-start | bytes 2162696 | tf_op jit(solution)/shard_map/ppermute | solution.py:17
  89.1 51.5 %collective-permute-start.22 = (bf16[256,1408]{1,0:T(8,128)(2,1)S(1)}, bf16[256,1408]{1,0:T(8,128)(2,1)S(1)}, u32[]{:S(2)}, u32[]{:S(2)}) collective-permute-start(bf16[256,1408]{1,0:T(8,128)(2,1)S(1)} %get-tuple-element.56), channel_id=1, source_target_pairs={{0,4},{4,0},{8,12},{12,8},{1,5},{5,1},{9,13},{13,9},{2,6},{6,2},{1... | collective-permute-start | bytes 2162696 | tf_op jit(solution)/shard_map/ppermute | solution.py:17
  90.8 47.8 %collective-permute-start.36 = (bf16[128,1408]{1,0:T(8,128)(2,1)S(1)}, bf16[128,1408]{1,0:T(8,128)(2,1)S(1)}, u32[]{:S(2)}, u32[]{:S(2)}) collective-permute-start(bf16[128,1408]{1,0:T(8,128)(2,1)S(1)} %get-tuple-element.58), channel_id=1, source_target_pairs={{0,4},{4,0},{8,12},{12,8},{1,5},{5,1},{9,13},{13,9},{2,6},{6,2},{1... | collective-permute-start | bytes 1081352 | tf_op jit(solution)/shard_map/ppermute | solution.py:17
  93.1 75.8 %collective-permute-start.24 = (bf16[256,1408]{1,0:T(8,128)(2,1)S(1)}, bf16[256,1408]{1,0:T(8,128)(2,1)S(1)}, u32[]{:S(2)}, u32[]{:S(2)}) collective-permute-start(bf16[256,1408]{1,0:T(8,128)(2,1)S(1)} %get-tuple-element.57), channel_id=1, source_target_pairs={{0,8},{4,12},{8,0},{12,4},{1,9},{5,13},{9,1},{13,5},{2,10},{6,14},... | collective-permute-start | bytes 2162696 | tf_op jit(solution)/shard_map/ppermute | solution.py:17
  138.6 27.6 %collective-permute-start.30 = (bf16[128,1408]{1,0:T(8,128)(2,1)S(1)}, bf16[128,1408]{1,0:T(8,128)(2,1)S(1)}, u32[]{:S(2)}, u32[]{:S(2)}) collective-permute-start(bf16[128,1408]{1,0:T(8,128)(2,1)S(1)} %get-tuple-element.64), channel_id=1, source_target_pairs={{0,8},{4,12},{8,0},{12,4},{1,9},{5,13},{9,1},{13,5},{2,10},{6,14},... | collective-permute-start | bytes 1081352 | tf_op jit(solution)/shard_map/ppermute | solution.py:17
  139.0 40.7 %collective-permute-start.21 = (bf16[256,1408]{1,0:T(8,128)(2,1)S(1)}, bf16[256,1408]{1,0:T(8,128)(2,1)S(1)}, u32[]{:S(2)}, u32[]{:S(2)}) collective-permute-start(bf16[256,1408]{1,0:T(8,128)(2,1)S(1)} %collective-permute-done.20.refs_3_), channel_id=1, source_target_pairs={{0,16},{16,0},{1,17},{17,1},{2,18},{18,2},{3,19},{19,3},{4,20},{20... | collective-permute-start | bytes 2162696 | tf_op jit(solution)/shard_map/ppermute | solution.py:17
  140.5 39.7 %collective-permute-start.23 = (bf16[256,1408]{1,0:T(8,128)(2,1)S(1)}, bf16[256,1408]{1,0:T(8,128)(2,1)S(1)}, u32[]{:S(2)}, u32[]{:S(2)}) collective-permute-start(bf16[256,1408]{1,0:T(8,128)(2,1)S(1)} %collective-permute-done.22.refs_5_), channel_id=1, source_target_pairs={{0,16},{16,0},{1,17},{17,1},{2,18},{18,2},{3,19},{19,3},{4,20},{20... | collective-permute-start | bytes 2162696 | tf_op jit(solution)/shard_map/ppermute | solution.py:17
  166.2 12.0 %collective-permute-start.26 = (bf16[128,1408]{1,0:T(8,128)(2,1)S(1)}, bf16[128,1408]{1,0:T(8,128)(2,1)S(1)}, u32[]{:S(2)}, u32[]{:S(2)}) collective-permute-start(bf16[128,1408]{1,0:T(8,128)(2,1)S(1)} %get-tuple-element.58), channel_id=1, source_target_pairs={{0,12},{4,8},{8,4},{12,0},{1,13},{5,9},{9,5},{13,1},{2,14},{6,10},... | collective-permute-start | bytes 1081352 | tf_op jit(solution)/shard_map/ppermute | solution.py:17
  168.8 20.1 %collective-permute-start.25 = (bf16[256,1408]{1,0:T(8,128)(2,1)S(1)}, bf16[256,1408]{1,0:T(8,128)(2,1)S(1)}, u32[]{:S(2)}, u32[]{:S(2)}) collective-permute-start(bf16[256,1408]{1,0:T(8,128)(2,1)S(1)} %collective-permute-done.24.refs_3_), channel_id=1, source_target_pairs={{0,16},{16,0},{1,17},{17,1},{2,18},{18,2},{3,19},{19,3},{4,20},{20... | collective-permute-start | bytes 2162696 | tf_op jit(solution)/shard_map/ppermute | solution.py:17
  178.2 18.5 %collective-permute-start.37 = (bf16[128,1408]{1,0:T(8,128)(2,1)S(1)}, bf16[128,1408]{1,0:T(8,128)(2,1)S(1)}, u32[]{:S(2)}, u32[]{:S(2)}) collective-permute-start(bf16[128,1408]{1,0:T(8,128)(2,1)S(1)} %collective-permute-done.36.refs_0_), channel_id=1, source_target_pairs={{0,16},{16,0},{1,17},{17,1},{2,18},{18,2},{3,19},{19,3},{4,20},{20... | collective-permute-start | bytes 1081352 | tf_op jit(solution)/shard_map/ppermute | solution.py:17
  179.7 24.7 %collective-permute-start.31 = (bf16[128,1408]{1,0:T(8,128)(2,1)S(1)}, bf16[128,1408]{1,0:T(8,128)(2,1)S(1)}, u32[]{:S(2)}, u32[]{:S(2)}) collective-permute-start(bf16[128,1408]{1,0:T(8,128)(2,1)S(1)} %collective-permute-done.30.refs_0_), channel_id=1, source_target_pairs={{0,16},{16,0},{1,17},{17,1},{2,18},{18,2},{3,19},{19,3},{4,20},{20... | collective-permute-start | bytes 1081352 | tf_op jit(solution)/shard_map/ppermute | solution.py:17
  180.2 30.5 %collective-permute-start.27 = (bf16[128,1408]{1,0:T(8,128)(2,1)S(1)}, bf16[128,1408]{1,0:T(8,128)(2,1)S(1)}, u32[]{:S(2)}, u32[]{:S(2)}) collective-permute-start(bf16[128,1408]{1,0:T(8,128)(2,1)S(1)} %collective-permute-done.26.refs_0_), channel_id=1, source_target_pairs={{0,16},{16,0},{1,17},{17,1},{2,18},{18,2},{3,19},{19,3},{4,20},{20... | collective-permute-start | bytes 1081352 | tf_op jit(solution)/shard_map/ppermute | solution.py:17
  192.5 20.2 %collective-permute-start.40 = (bf16[512,512]{1,0:T(8,128)(2,1)S(1)}, bf16[512,512]{1,0:T(8,128)(2,1)S(1)}, u32[]{:S(2)}, u32[]{:S(2)}) collective-permute-start(bf16[512,512]{1,0:T(8,128)(2,1)S(1)} %get-tuple-element.79), channel_id=1, source_target_pairs={{0,1},{1,0},{2,3},{3,2},{4,5},{5,4},{6,7},{7,6},{8,9},{9,8},{10,11... | collective-permute-start | bytes 1572872 | tf_op jit(solution)/shard_map/ppermute | solution.py:17
  198.5 15.8 %collective-permute-start.38 = (bf16[512,512]{1,0:T(8,128)(2,1)S(1)}, bf16[512,512]{1,0:T(8,128)(2,1)S(1)}, u32[]{:S(2)}, u32[]{:S(2)}) collective-permute-start(bf16[512,512]{1,0:T(8,128)(2,1)S(1)} %get-tuple-element.73), channel_id=1, source_target_pairs={{0,1},{1,0},{2,3},{3,2},{4,5},{5,4},{6,7},{7,6},{8,9},{9,8},{10,11... | collective-permute-start | bytes 1572872 | tf_op jit(solution)/shard_map/ppermute | solution.py:17
  214.4 13.2 %collective-permute-start.39 = (bf16[256,512]{1,0:T(8,128)(2,1)S(1)}, bf16[256,512]{1,0:T(8,128)(2,1)S(1)}, u32[]{:S(2)}, u32[]{:S(2)}) collective-permute-start(bf16[256,512]{1,0:T(8,128)(2,1)S(1)} %get-tuple-element.75), channel_id=1, source_target_pairs={{0,2},{1,3},{2,0},{3,1},{4,6},{5,7},{6,4},{7,5},{8,10},{9,11},{10,... | collective-permute-start | bytes 786440 | tf_op jit(solution)/shard_map/ppermute | solution.py:17
  215.2 18.1 %collective-permute-start.33 = (bf16[256,512]{1,0:T(8,128)(2,1)S(1)}, bf16[256,512]{1,0:T(8,128)(2,1)S(1)}, u32[]{:S(2)}, u32[]{:S(2)}) collective-permute-start(bf16[256,512]{1,0:T(8,128)(2,1)S(1)} %get-tuple-element.68), channel_id=1, source_target_pairs={{0,2},{1,3},{2,0},{3,1},{4,6},{5,7},{6,4},{7,5},{8,10},{9,11},{10,... | collective-permute-start | bytes 786440 | tf_op jit(solution)/shard_map/ppermute | solution.py:17
  216.9 21.6 %collective-permute-start.29 = (bf16[256,512]{1,0:T(8,128)(2,1)S(1)}, bf16[256,512]{1,0:T(8,128)(2,1)S(1)}, u32[]{:S(2)}, u32[]{:S(2)}) collective-permute-start(bf16[256,512]{1,0:T(8,128)(2,1)S(1)} %get-tuple-element.62), channel_id=1, source_target_pairs={{0,2},{1,3},{2,0},{3,1},{4,6},{5,7},{6,4},{7,5},{8,10},{9,11},{10,... | collective-permute-start | bytes 786440 | tf_op jit(solution)/shard_map/ppermute | solution.py:17
  222.1 18.3 %collective-permute-start.42 = (bf16[128,512]{1,0:T(8,128)(2,1)S(1)}, bf16[128,512]{1,0:T(8,128)(2,1)S(1)}, u32[]{:S(2)}, u32[]{:S(2)}) collective-permute-start(bf16[128,512]{1,0:T(8,128)(2,1)S(1)} %get-tuple-element.82), channel_id=1, source_target_pairs={{0,4},{4,0},{8,12},{12,8},{1,5},{5,1},{9,13},{13,9},{2,6},{6,2},{1... | collective-permute-start | bytes 393224 | tf_op jit(solution)/shard_map/ppermute | solution.py:17
  227.7 12.7 %collective-permute-start.43 = (bf16[128,512]{1,0:T(8,128)(2,1)S(1)}, bf16[128,512]{1,0:T(8,128)(2,1)S(1)}, u32[]{:S(2)}, u32[]{:S(2)}) collective-permute-start(bf16[128,512]{1,0:T(8,128)(2,1)S(1)} %get-tuple-element.84), channel_id=1, source_target_pairs={{0,4},{4,0},{8,12},{12,8},{1,5},{5,1},{9,13},{13,9},{2,6},{6,2},{1... | collective-permute-start | bytes 393224 | tf_op jit(solution)/shard_map/ppermute | solution.py:17
  (23 other events, 198.4 us)
